TPU v7x, 1024 devices: a whole 4x8x16 slice. The times are simulated.
1024 devices in a mesh: ep: 32 (over z, core), tp: 32 (over y, x).
Axes of the slice: x: 4, y: 8, z: 16, core: 2. Of those that a mesh axis runs over, the one named last changes fastest.
Arguments:
- tokens: bfloat16 [2048, 4096], P('ep', 'tp'), may hold values from -600 to 600
- in_gain: float32 [4096], P('tp'), may hold values from 0.1 to 1.9
- out_gain: float32 [4096], P('tp'), may hold values from 0.1 to 1.9
- routes: int32 [2048, 4], replicated, may hold values from 0 to 127, as said below
- route_weights: float32 [2048, 4], replicated, may hold values from 0.05 to 1
- w_gate: bfloat16 [128, 4096, 1024], P('ep', 'tp'), may hold values from -0.09375 to 0.09375
- w_up: bfloat16 [128, 4096, 1024], P('ep', 'tp'), may hold values from -0.09375 to 0.09375
- w_down: bfloat16 [128, 1024, 4096], P('ep', None, 'tp'), may hold values from -0.375 to 0.375
Outputs:
- result: bfloat16 [2048, 4096], P('ep', 'tp')
Inputs may be any that keep to these rules, and one draw needn't show every extreme that they name: `routes`: each row names 4 different experts, all in one group of 8 consecutive numbers. In the rows of one index of ep (aligned blocks of 64 rows) no expert is named by more than 4 rows, and some expert by exactly 4.
All inputs are finite; a program needn't handle non-finite values.
Results may differ from a plain program's by a relative error of at most 0.025.
Values may be sent and summed in bfloat16 or wider, within the bound.
No kernel may reach another device: no remote copies, remote signals or barrier semaphores. Data moves between devices by JAX's collectives and lax.ppermute only.
A program may use at most 32 MiB of HBM per device.

v0:
```python
import jax
import jax.numpy as jnp
from jax import lax
from jax.experimental import pallas as pl
from jax.experimental.pallas import tpu as pltpu
from jax.sharding import Mesh, PartitionSpec as P

EPS = 1e-06
BF, F32 = jnp.bfloat16, jnp.float32
LANES = 128
HALF = 64
CAP = 4
GROUP = 8
PIECES = 1
PARAMS = pltpu.CompilerParams(vmem_limit_bytes=16 * 1024 * 1024)
FIRST = {"z": lambda n: 13, "c": lambda n: n - 1, "y": lambda n: n // 2, "x": lambda n: n // 2}
STEP = {"z": 1, "c": 1, "y": 1, "x": 1}
REDUCE = [4, 7, 2, 5, 0, 3, 6, 1]
GATHER = [4, 7, 2, 5, 0, 3, 6, 1]
VMEM = pl.BlockSpec(memory_space=pltpu.VMEM)
HBM = pl.BlockSpec(memory_space=pltpu.HBM)


def in_hbm(value):
    return pltpu.with_memory_space_constraint(value, pltpu.HBM)


def shape(dims, dtype):
    return jax.ShapeDtypeStruct(dims, dtype)


def iota(dims, dim):
    return lax.broadcasted_iota(jnp.int32, dims, dim)


def ones_where(mask, dtype=BF):
    return jnp.where(mask, 1.0, 0.0).astype(dtype)


def earlier():
    s, t = iota((LANES, LANES), 0), iota((LANES, LANES), 1)
    return ones_where((s < t) & ((s >> 6) == (t >> 6)))


def dot(a, b):
    return jnp.dot(a, b, preferred_element_type=F32)


def dot_rows(a, b):
    return lax.dot_general(a, b, (((0,), (0,)), ((), ())), preferred_element_type=F32)


def call(kernel, outs, *args):
    single = not isinstance(outs, (list, tuple))
    return pl.pallas_call(
        kernel,
        out_shape=outs,
        in_specs=[VMEM] * len(args),
        out_specs=VMEM if single else [VMEM] * len(outs),
        compiler_params=PARAMS,
    )(*args)


def place_of(index, axis):
    n = lax.axis_size(axis)
    return lax.rem(index + n - FIRST[axis](n), n)


def named(ids, expert):
    hit = ids[0] == expert
    for k in range(1, CAP):
        hit = hit | (ids[k] == expert)
    return jnp.where(hit, 1.0, 0.0)


def slice_copies(sources, outs, shifts, sems):
    x = lax.axis_index("x")
    copies = []
    for d, out in zip(shifts, outs):
        for i, source in enumerate(sources):
            at = lax.rem(x + d, source.shape[0])
            rows = source.shape[1] // PIECES
            for k in range(PIECES):
                part = pl.ds(k * rows, rows)
                copies.append(
                    pltpu.make_async_copy(
                        source.at[at, part, :], out.at[i, part, :], sems.at[len(copies)]
                    )
                )
    return copies


def deal(arrays, shifts, kernel=None, extra=(), extra_outs=()):
    one = shape((len(arrays), *arrays[0].shape[1:]), BF)
    n, m, k = len(arrays), len(shifts), len(extra)

    def body(*refs):
        sources, small, rest = refs[:n], refs[n : n + k], refs[n + k :]
        outs, held, sems, small_sems = rest[: len(rest) - k - 2], rest[-k - 2 : -2], *rest[-2:]
        fetches = [
            pltpu.make_async_copy(small[i], held[i], small_sems.at[i]) for i in range(k)
        ]
        copies = slice_copies(sources, outs[:m], shifts, sems)
        for copy in fetches + copies:
            copy.start()
        for copy in fetches:
            copy.wait()
        if kernel is not None:
            kernel(*held, *outs[m:])
        for copy in copies:
            copy.wait()

    return pl.pallas_call(
        body,
        out_shape=[one] * m + list(extra_outs),
        in_specs=[HBM] * (n + k),
        out_specs=[VMEM] * (m + len(extra_outs)),
        scratch_shapes=[pltpu.VMEM(a.shape, a.dtype) for a in extra]
        + [pltpu.SemaphoreType.DMA((m * n * PIECES,)), pltpu.SemaphoreType.DMA((max(k, 1),))],
        compiler_params=PARAMS,
    )(*[in_hbm(a) for a in (*arrays, *extra)])


def dispatch(ids, tok_ref, out_ref, place_ref):
    z, c = lax.axis_index("z"), lax.axis_index("c")
    chips = ids[0].shape[0]
    first = jnp.sum(jnp.where(iota(ids[0].shape, 0) == z, ids[0], 0), axis=0, keepdims=True)
    group = first >> 3
    member = iota((chips, LANES), 0) == group
    rank = dot(ones_where(member), earlier())
    rank = jnp.sum(jnp.where(member, rank, 0.0), axis=0, keepdims=True).astype(jnp.int32)
    mine = (iota((1, LANES), 1) >> 6) == c
    row = jnp.where(mine, place_of(group, "z") * GROUP + rank, -1)
    place = ones_where(iota((LANES, LANES), 0) == row)
    place_ref[...] = place
    tok = tok_ref[...]
    out_ref[...] = dot(place, jnp.concatenate([tok, tok], axis=0)).astype(BF)


def select_table(ids, sel_ref):
    z, c = lax.axis_index("z"), lax.axis_index("c")
    chips = ids[0].shape[0]
    before = earlier()
    rows = [named(ids, z * GROUP + e) for e in listed(("c", "x"))]
    hits = jnp.concatenate(rows, axis=0)
    anyone = rows[0]
    for e in range(1, GROUP):
        anyone = jnp.maximum(anyone, rows[e])
    rank = dot(hits.astype(BF), before)
    start = (place_of(iota((chips, LANES), 0), "z") * GROUP).astype(F32)
    spot = dot(anyone.astype(BF), before) + start
    spots = jnp.concatenate([spot] * GROUP, axis=0)
    lane = iota((LANES, LANES), 1).astype(F32)
    live = (hits > 0.0) & ((iota((LANES, LANES), 1) >> 6) == c)
    for q in range(CAP):
        at = jnp.sum(jnp.where(live & (rank == q), spots + 1.0, 0.0), axis=1, keepdims=True) - 1.0
        sel_ref[q] = ones_where(lane == at)


def slot_scales(ids, weights_ref, scale_ref):
    z, c, x = lax.axis_index("z"), lax.axis_index("c"), lax.axis_index("x")
    chips = ids[0].shape[0]
    own = z * GROUP + c * CAP + x
    hit = named(ids, own)
    rank = dot(hit.astype(BF), earlier())
    weight = jnp.zeros((chips, LANES), F32)
    for k in range(CAP):
        weight = weight + jnp.where(ids[k] == own, weights_ref[:, k, :], 0.0)
    block = iota((chips, LANES), 1) >> 6
    for i, core in enumerate(listed(("c",))):
        for q in range(CAP):
            at = (hit > 0.0) & (rank == q) & (block == core)
            value = jnp.sum(jnp.where(at, weight, 0.0), axis=1, keepdims=True)
            start = (i * CAP + q) * chips
            scale_ref[start : start + chips, :] = jnp.broadcast_to(value, (chips, LANES))


def three_rows(gain, tail_ref):
    high = gain.astype(BF).astype(F32)
    middle = (gain - high).astype(BF).astype(F32)
    low = gain - high - middle
    row = iota((8, LANES), 0)
    tail = jnp.where(row == 0, high, jnp.where(row == 1, middle, jnp.where(row == 2, low, 0.0)))
    tail_ref[...] = tail.astype(BF)


def routing_kernel(
    routes_ref, weights_ref, tok_ref, gain_ref, last_ref,
    out_ref, place_ref, sel_ref, tail_ref, scale_ref, last_out_ref,
):
    ids = [routes_ref[:, k, :] for k in range(CAP)]
    dispatch(ids, tok_ref, out_ref, place_ref)
    select_table(ids, sel_ref)
    three_rows(gain_ref[...], tail_ref)
    slot_scales(ids, weights_ref, scale_ref)
    last_out_ref[...] = jnp.broadcast_to(last_ref[...], last_out_ref.shape)


def passed(piece, d, axis):
    n = lax.axis_size(axis)
    return lax.ppermute(piece, axis, [(i, (i + d) % n) for i in range(n)])


def mark_kernel(in_ref, out_ref):
    out_ref[...] = in_ref[...]


def select_kernel(recv_ref, sel_ref, tail_ref, out_ref):
    recv = recv_ref[...]
    for q in range(CAP):
        picked = dot(sel_ref[q], recv).astype(BF)
        for e in range(GROUP):
            out_ref[e, q * 16 : (q + 1) * 16, :] = picked[e * 16 : (e + 1) * 16]
    tail = tail_ref[...]
    for e in range(GROUP):
        out_ref[e, 64:72, :] = tail


def gate_up_kernel(rows_ref, *refs):
    *weights, out_ref = refs
    n = len(weights)
    x = lax.axis_index("x")
    squares = jnp.zeros((LANES, 1), F32)
    hidden = weights[0].shape[2]
    gate = jnp.zeros((LANES, hidden), F32)
    up = jnp.zeros((LANES, hidden), F32)
    for d in range(n):
        at = place_of(x - d + n, "x")
        raw = jnp.concatenate([rows_ref[at, 0:64, :], rows_ref[n + at, 0:64, :]], axis=0)
        raw = raw.astype(F32)
        tail = rows_ref[at, 64:72, :].astype(F32)
        gain = tail[0:1] + tail[1:2] + tail[2:3]
        squares = squares + jnp.sum(raw * raw, axis=1, keepdims=True)
        lhs = (raw * gain).astype(BF)
        gate = gate + dot(lhs, weights[d][0])
        up = up + dot(lhs, weights[d][1])
    out_ref[:, 0:hidden] = gate.astype(BF)
    out_ref[:, hidden : 2 * hidden] = up.astype(BF)
    high = squares.astype(BF).astype(F32)
    lane = iota((LANES, LANES), 1)
    out_ref[:, 2 * hidden :] = jnp.where(lane < HALF, high, squares - high).astype(BF)


def act_kernel(width, parts_ref, out_ref):
    total = parts_ref[0].astype(F32)
    for y in range(1, parts_ref.shape[0]):
        total = total + parts_ref[y].astype(F32)
    hidden = out_ref.shape[2]
    squares = total[:, 2 * hidden : 2 * hidden + 1] + total[:, 2 * hidden + HALF : 2 * hidden + HALF + 1]
    scale = lax.rsqrt(squares / width + EPS)
    gate = total[:, 0:hidden] * scale
    up = total[:, hidden : 2 * hidden] * scale
    act = (gate / (1.0 + jnp.exp(-gate)) * up).astype(BF)
    for y in range(out_ref.shape[0]):
        out_ref[y] = act


def down_kernel(act_ref, scale_ref, *refs):
    *weights, out_ref = refs
    n = len(weights)
    x = lax.axis_index("x")
    rows = act_ref.shape[0] // len(GATHER)
    at = [GATHER.index(y) * rows for y in REDUCE]
    act = jnp.concatenate([act_ref[i : i + rows, :] for i in at], axis=0)
    scale = scale_ref[...]
    for d in range(n):
        at = place_of(x - d + n, "x")
        out = (dot(act, weights[d][0]) * scale).astype(BF)
        out_ref[at] = out[0:64]
        out_ref[n + at] = out[64:128]


def combine_kernel(parts_ref, sel_ref, out_ref):
    total = jnp.zeros((LANES, LANES), F32)
    for q in range(CAP):
        rows = jnp.concatenate(
            [parts_ref[e, q * 16 : (q + 1) * 16, :] for e in range(GROUP)], axis=0
        )
        total = total + dot_rows(sel_ref[q], rows)
    out_ref[...] = total.astype(BF)


def place_kernel(ret_ref, place_ref, comb_ref, squares_ref):
    full = dot_rows(place_ref[...], ret_ref[...])
    comb_ref[...] = full[0:HALF] + full[HALF:LANES]
    squares = jnp.sum(full * full, axis=1, keepdims=True)
    flat = jnp.transpose(jnp.broadcast_to(squares, (LANES, LANES)))[0:1, :]
    for i in range(squares_ref.shape[0]):
        squares_ref[i] = flat


def norm_kernel(width, squares_ref, comb_ref, gain_ref, out_ref):
    total = squares_ref[0]
    for i in range(1, squares_ref.shape[0]):
        total = total + squares_ref[i]
    column = jnp.transpose(jnp.broadcast_to(total, (LANES, LANES)))
    column = column[0:HALF] + column[HALF:LANES]
    out_ref[...] = (comb_ref[...] * lax.rsqrt(column / width + EPS) * gain_ref[0:1, :]).astype(BF)


def listed(axes):
    order = [0]
    for axis in axes:
        n = lax.axis_size(axis)
        order = [i * n + (FIRST[axis](n) + STEP[axis] * k) % n for i in order for k in range(n)]
    return order


def exchange(value, axes, order=None):
    groups = [listed(axes) if order is None else order]
    return lax.all_to_all(value, axes, 0, 0, tiled=True, axis_index_groups=groups)


def on_device(tokens, in_gain, out_gain, routes, route_weights, w_gate, w_up, w_down):
    chips, ys, xs = lax.axis_size("z"), lax.axis_size("y"), lax.axis_size("x")
    local = tokens.shape[1]
    width = float(local * ys * xs)
    hidden = w_gate.shape[2]
    routes = jnp.transpose(routes.reshape(chips, LANES, CAP), (0, 2, 1))
    weights = jnp.transpose(route_weights.reshape(chips, LANES, CAP), (0, 2, 1))

    square = shape((LANES, LANES), BF)
    own, near, far, back, outgoing, place, sel, tail, scale, last_gain = deal(
        [w_gate, w_up],
        [0, 1, 2, 3],
        routing_kernel,
        (routes, weights, tokens, in_gain.reshape(1, local), out_gain.reshape(1, local)),
        (
            square,
            square,
            shape((CAP, LANES, LANES), BF),
            shape((8, LANES), BF),
            shape((LANES, LANES), F32),
            shape((8, LANES), F32),
        ),
    )
    gate_up = [own, passed(near, 1, "x"), passed(far, 2, "x"), passed(back, 3, "x")]
    own, near, far, back = deal([w_down], [0, 1, 2, 3])
    down = [own, passed(near, 1, "x"), passed(far, 2, "x"), passed(back, 3, "x")]
    arrived = exchange(outgoing.reshape(chips, GROUP, local), ("z",))
    slots = call(
        select_kernel, shape((GROUP, 72, LANES), BF), arrived.reshape(LANES, local), sel, tail
    )
    slots = exchange(slots, ("c", "x"))
    parts = call(gate_up_kernel, shape((LANES, 2 * hidden + LANES), BF), slots, *gate_up)
    last_gain = call(mark_kernel, shape((8, LANES), F32), last_gain)
    parts = exchange(parts.reshape(ys, LANES // ys, 2 * hidden + LANES), ("y",), REDUCE)
    act = call(lambda *refs: act_kernel(width, *refs), shape((ys, LANES // ys, hidden), BF), parts)
    act = exchange(act, ("y",), GATHER).reshape(LANES, hidden)
    answers = call(down_kernel, shape((GROUP, 64, LANES), BF), act, scale, *down)
    answers = exchange(answers, ("c", "x"))
    mixed = call(combine_kernel, shape((LANES, local), BF), answers, sel)
    returned = exchange(mixed.reshape(chips, GROUP, local), ("z",))
    combined, squares = call(
        place_kernel,
        [shape((HALF, local), F32), shape((ys * xs, 1, LANES), F32)],
        returned.reshape(LANES, local),
        place,
    )
    squares = exchange(squares, ("y", "x"))
    return call(
        lambda *refs: norm_kernel(width, *refs),
        shape((HALF, local), BF),
        squares,
        combined,
        last_gain,
    )


def solution(mesh):
    fine = Mesh(
        mesh.devices.reshape(mesh.shape["ep"] // 2, 2, mesh.shape["tp"] // 4, 4),
        ("z", "c", "y", "x"),
    )
    ep, tp = ("z", "c"), ("y", "x")
    placed = (
        P(ep, tp),
        P(tp),
        P(tp),
        P(),
        P(),
        P(ep, tp, None),
        P(ep, tp, None),
        P(ep, None, tp),
    )

    return jax.shard_map(on_device, mesh=fine, in_specs=placed, out_specs=P(ep, tp), check_vma=False)
```

profile of v0, /device:TPU:2, one launch (start us, length us, event | category | flops | bytes accessed | tf_op | source)
XLA Modules:
  0.0 137.5 jit_solution(15343367871533846143)
XLA Ops:
  0.0 2.1 %shard_map.82 = (bf16[2,128,1024]{2,1,0:T(8,128)(2,1)S(1)}, bf16[2,128,1024]{2,1,0:T(8,128)(2,1)S(1)}, bf16[2,128,1024]{2,1,0:T(8,128)(2,1)S(1)}, bf16[2,128,102...) custom-call(bf16[4,128,1024]{2,1,0:T(8,128)(2,1)} %refs_0_.2, ...), custom_call_target="tpu_custom_call" | custom-call | tf_op jit(solution)/shard_map/pallas_call | solution.py:113
  2.1 3.4 %collective-permute-start = (bf16[2,128,1024]{2,1,0:T(8,128)(2,1)S(1)}, bf16[2,128,1024]{2,1,0:T(8,128)(2,1)S(1)}, u32[]{:S(2)}, u32[]{:S(2)}) collective-permute-start(bf16[2,128,1024]{2,1,0:T(8,128)(2,1)S(1)} %get-tuple-element.25), channel_id=1, source_target_pairs={{0,1},{1,2},{2,3},{3,0},{4,5},{5,6},{6,7},{7,4},{8,9},{9,10},{10,1... | collective-permute-start | bytes 1572872 | tf_op jit(solution)/shard_map/ppermute | solution.py:201
  5.5 15.6 %collective-permute-start.1 = (bf16[2,128,1024]{2,1,0:T(8,128)(2,1)S(1)}, bf16[2,128,1024]{2,1,0:T(8,128)(2,1)S(1)}, u32[]{:S(2)}, u32[]{:S(2)}) collective-permute-start(bf16[2,128,1024]{2,1,0:T(8,128)(2,1)S(1)} %get-tuple-element.26), channel_id=1, source_target_pairs={{0,2},{1,3},{2,0},{3,1},{4,6},{5,7},{6,4},{7,5},{8,10},{9,11},{10,... | collective-permute-start | bytes 1572872 | tf_op jit(solution)/shard_map/ppermute | solution.py:201
  21.1 1.9 %collective-permute-start.2 = (bf16[2,128,1024]{2,1,0:T(8,128)(2,1)S(1)}, bf16[2,128,1024]{2,1,0:T(8,128)(2,1)S(1)}, u32[]{:S(2)}, u32[]{:S(2)}) collective-permute-start(bf16[2,128,1024]{2,1,0:T(8,128)(2,1)S(1)} %get-tuple-element.27), channel_id=1, source_target_pairs={{0,3},{1,0},{2,1},{3,2},{4,7},{5,4},{6,5},{7,6},{8,11},{9,8},{10,9... | collective-permute-start | bytes 1572872 | tf_op jit(solution)/shard_map/ppermute | solution.py:201
  23.0 17.9 %all_to_all.35 = bf16[16,8,128]{2,1,0:T(8,128)(2,1)S(1)} all-to-all(bf16[16,8,128]{2,1,0:T(8,128)(2,1)S(1)} %bitcast.19), channel_id=1, replica_groups={{832,896,960,0,64,128,192,256,320,384,448,512,576,640,704,768},{833,897..., dimensions={0} | all-to-all | bytes 65536 | tf_op jit(solution)/shard_map/all_to_all | solution.py:311
  40.9 0.2 shard_map.83
  41.1 8.5 %all_to_all.36.rows_ref = bf16[8,72,128]{2,1,0:T(8,128)(2,1)S(1)} all-to-all(bf16[8,72,128]{2,1,0:T(8,128)(2,1)S(1)} %shard_map.83), channel_id=1, replica_groups={{34,35,32,33,2,3,0,1},{38,39,36,37,6,7,4,5},{42,43,40,41,10,11,8,9},{46..., dimensions={0} | all-to-all | bytes 294912 | tf_op jit(solution)/shard_map/all_to_all | solution.py:311
  49.6 0.0 collective-permute-done.refs_1_
  49.6 0.0 collective-permute-done.1.refs_2_
  49.6 0.0 collective-permute-done.2.refs_3_
  49.6 0.7 shard_map.84
  50.3 21.1 %all_to_all.37.refs_0_ = bf16[8,16,2176]{2,1,0:T(8,128)(2,1)S(1)} all-to-all(bf16[8,16,2176]{2,1,0:T(8,128)(2,1)S(1)} %bitcast.14), channel_id=1, replica_groups={{16,28,8,20,0,12,24,4},{17,29,9,21,1,13,25,5},{18,30,10,22,2,14,26,6},{..., dimensions={0} | all-to-all | bytes 1114112 | tf_op jit(solution)/shard_map/all_to_all | solution.py:311
  71.4 0.9 shard_map.85
  72.3 8.6 %all-to-all-start.3 = ((bf16[8,16,1024]{2,1,0:T(8,128)(2,1)}), bf16[8,16,1024]{2,1,0:T(8,128)(2,1)S(1)}, u32[]{:S(2)}, u32[]{:S(2)}) async-start(bf16[8,16,1024]{2,1,0:T(8,128)(2,1)} %shard_map.85), calls=%async_computation.3 | async-start | bytes 524288 | tf_op jit(solution)/shard_map/all_to_all | solution.py:311
  80.9 1.2 shard_map.86
  82.2 3.3 %collective-permute-start.3 = (bf16[1,1024,128]{2,1,0:T(8,128)(2,1)S(1)}, bf16[1,1024,128]{2,1,0:T(8,128)(2,1)S(1)}, u32[]{:S(2)}, u32[]{:S(2)}) collective-permute-start(bf16[1,1024,128]{2,1,0:T(8,128)(2,1)S(1)} %get-tuple-element.30), channel_id=1, source_target_pairs={{0,1},{1,2},{2,3},{3,0},{4,5},{5,6},{6,7},{7,4},{8,9},{9,10},{10,1... | collective-permute-start | bytes 786440 | tf_op jit(solution)/shard_map/ppermute | solution.py:201
  85.4 3.0 %collective-permute-start.4 = (bf16[1,1024,128]{2,1,0:T(8,128)(2,1)S(1)}, bf16[1,1024,128]{2,1,0:T(8,128)(2,1)S(1)}, u32[]{:S(2)}, u32[]{:S(2)}) collective-permute-start(bf16[1,1024,128]{2,1,0:T(8,128)(2,1)S(1)} %get-tuple-element.31), channel_id=1, source_target_pairs={{0,2},{1,3},{2,0},{3,1},{4,6},{5,7},{6,4},{7,5},{8,10},{9,11},{10,... | collective-permute-start | bytes 786440 | tf_op jit(solution)/shard_map/ppermute | solution.py:201
  88.5 4.3 %collective-permute-start.5 = (bf16[1,1024,128]{2,1,0:T(8,128)(2,1)S(1)}, bf16[1,1024,128]{2,1,0:T(8,128)(2,1)S(1)}, u32[]{:S(2)}, u32[]{:S(2)}) collective-permute-start(bf16[1,1024,128]{2,1,0:T(8,128)(2,1)S(1)} %get-tuple-element.32), channel_id=1, source_target_pairs={{0,3},{1,0},{2,1},{3,2},{4,7},{5,4},{6,5},{7,6},{8,11},{9,8},{10,9... | collective-permute-start | bytes 786440 | tf_op jit(solution)/shard_map/ppermute | solution.py:201
  92.7 0.0 collective-permute-done.3.refs_1_
  92.7 4.8 %collective-permute-done.4.refs_2_ = bf16[1,1024,128]{2,1,0:T(8,128)(2,1)S(1)} collective-permute-done((bf16[1,1024,128]{2,1,0:T(8,128)(2,1)S(1)}, bf16[1,1024,128]{2,1,0:T(8,128)(2,1)S(1)}, u32[]{:S(2)}, u32[]{:S(2)}) %collective-permute-start.4) | collective-permute-done | bytes 262176 | tf_op jit(solution)/shard_map/ppermute | solution.py:201
  97.5 2.7 %collective-permute-done.5.refs_3_ = bf16[1,1024,128]{2,1,0:T(8,128)(2,1)S(1)} collective-permute-done((bf16[1,1024,128]{2,1,0:T(8,128)(2,1)S(1)}, bf16[1,1024,128]{2,1,0:T(8,128)(2,1)S(1)}, u32[]{:S(2)}, u32[]{:S(2)}) %collective-permute-start.5) | collective-permute-done | bytes 262176 | tf_op jit(solution)/shard_map/ppermute | solution.py:201
  100.2 0.0 all-to-all-done.3
  100.2 0.4 shard_map.87
  100.7 7.7 %all_to_all.38.parts_ref = bf16[8,64,128]{2,1,0:T(8,128)(2,1)S(1)} all-to-all(bf16[8,64,128]{2,1,0:T(8,128)(2,1)S(1)} %shard_map.87), channel_id=1, replica_groups={{34,35,32,33,2,3,0,1},{38,39,36,37,6,7,4,5},{42,43,40,41,10,11,8,9},{46..., dimensions={0} | all-to-all | bytes 262144 | tf_op jit(solution)/shard_map/all_to_all | solution.py:311
  108.4 0.2 shard_map.88
  108.6 15.0 %all_to_all.39 = bf16[16,8,128]{2,1,0:T(8,128)(2,1)S(1)} all-to-all(bf16[16,8,128]{2,1,0:T(8,128)(2,1)S(1)} %bitcast.17), channel_id=1, replica_groups={{832,896,960,0,64,128,192,256,320,384,448,512,576,640,704,768},{833,897..., dimensions={0} | all-to-all | bytes 65536 | tf_op jit(solution)/shard_map/all_to_all | solution.py:311
  123.5 0.9 shard_map.89
  124.5 8.5 %all-to-all-start.6 = ((f32[32,1,128]{2,1,0:T(1,128)}), f32[32,1,128]{2,1,0:T(1,128)S(1)}, u32[]{:S(2)}, u32[]{:S(2)}) async-start(f32[32,1,128]{2,1,0:T(1,128)} %get-tuple-element.34), calls=%async_computation.6 | async-start | bytes 32768 | tf_op jit(solution)/shard_map/all_to_all | solution.py:311
  133.0 3.8 %all-to-all-done.6.refs_0_ = f32[32,1,128]{2,1,0:T(1,128)S(1)} async-done(((f32[32,1,128]{2,1,0:T(1,128)}), f32[32,1,128]{2,1,0:T(1,128)S(1)}, u32[]{:S(2)}, u32[]{:S(2)}) %all-to-all-start.6) | async-done | bytes 16416 | tf_op jit(solution)/shard_map/all_to_all | solution.py:311
  136.7 0.8 shard_map.91
  (1 shorter events, 0.0 us)
Async XLA Ops:
  2.1 47.6 %collective-permute-start = (bf16[2,128,1024]{2,1,0:T(8,128)(2,1)S(1)}, bf16[2,128,1024]{2,1,0:T(8,128)(2,1)S(1)}, u32[]{:S(2)}, u32[]{:S(2)}) collective-permute-start(bf16[2,128,1024]{2,1,0:T(8,128)(2,1)S(1)} %get-tuple-element.25), channel_id=1, source_target_pairs={{0,1},{1,2},{2,3},{3,0},{4,5},{5,6},{6,7},{7,4},{8,9},{9,10},{10,1... | collective-permute-start | bytes 1572872 | tf_op jit(solution)/shard_map/ppermute | solution.py:201
  5.5 44.2 %collective-permute-start.1 = (bf16[2,128,1024]{2,1,0:T(8,128)(2,1)S(1)}, bf16[2,128,1024]{2,1,0:T(8,128)(2,1)S(1)}, u32[]{:S(2)}, u32[]{:S(2)}) collective-permute-start(bf16[2,128,1024]{2,1,0:T(8,128)(2,1)S(1)} %get-tuple-element.26), channel_id=1, source_target_pairs={{0,2},{1,3},{2,0},{3,1},{4,6},{5,7},{6,4},{7,5},{8,10},{9,11},{10,... | collective-permute-start | bytes 1572872 | tf_op jit(solution)/shard_map/ppermute | solution.py:201
  21.1 28.5 %collective-permute-start.2 = (bf16[2,128,1024]{2,1,0:T(8,128)(2,1)S(1)}, bf16[2,128,1024]{2,1,0:T(8,128)(2,1)S(1)}, u32[]{:S(2)}, u32[]{:S(2)}) collective-permute-start(bf16[2,128,1024]{2,1,0:T(8,128)(2,1)S(1)} %get-tuple-element.27), channel_id=1, source_target_pairs={{0,3},{1,0},{2,1},{3,2},{4,7},{5,4},{6,5},{7,6},{8,11},{9,8},{10,9... | collective-permute-start | bytes 1572872 | tf_op jit(solution)/shard_map/ppermute | solution.py:201
  72.3 27.9 %all-to-all-start.3 = ((bf16[8,16,1024]{2,1,0:T(8,128)(2,1)}), bf16[8,16,1024]{2,1,0:T(8,128)(2,1)S(1)}, u32[]{:S(2)}, u32[]{:S(2)}) async-start(bf16[8,16,1024]{2,1,0:T(8,128)(2,1)} %shard_map.85), calls=%async_computation.3 | async-start | bytes 524288 | tf_op jit(solution)/shard_map/all_to_all | solution.py:311
  82.2 10.5 %collective-permute-start.3 = (bf16[1,1024,128]{2,1,0:T(8,128)(2,1)S(1)}, bf16[1,1024,128]{2,1,0:T(8,128)(2,1)S(1)}, u32[]{:S(2)}, u32[]{:S(2)}) collective-permute-start(bf16[1,1024,128]{2,1,0:T(8,128)(2,1)S(1)} %get-tuple-element.30), channel_id=1, source_target_pairs={{0,1},{1,2},{2,3},{3,0},{4,5},{5,6},{6,7},{7,4},{8,9},{9,10},{10,1... | collective-permute-start | bytes 786440 | tf_op jit(solution)/shard_map/ppermute | solution.py:201
  85.4 12.1 %collective-permute-start.4 = (bf16[1,1024,128]{2,1,0:T(8,128)(2,1)S(1)}, bf16[1,1024,128]{2,1,0:T(8,128)(2,1)S(1)}, u32[]{:S(2)}, u32[]{:S(2)}) collective-permute-start(bf16[1,1024,128]{2,1,0:T(8,128)(2,1)S(1)} %get-tuple-element.31), channel_id=1, source_target_pairs={{0,2},{1,3},{2,0},{3,1},{4,6},{5,7},{6,4},{7,5},{8,10},{9,11},{10,... | collective-permute-start | bytes 786440 | tf_op jit(solution)/shard_map/ppermute | solution.py:201
  88.5 11.8 %collective-permute-start.5 = (bf16[1,1024,128]{2,1,0:T(8,128)(2,1)S(1)}, bf16[1,1024,128]{2,1,0:T(8,128)(2,1)S(1)}, u32[]{:S(2)}, u32[]{:S(2)}) collective-permute-start(bf16[1,1024,128]{2,1,0:T(8,128)(2,1)S(1)} %get-tuple-element.32), channel_id=1, source_target_pairs={{0,3},{1,0},{2,1},{3,2},{4,7},{5,4},{6,5},{7,6},{8,11},{9,8},{10,9... | collective-permute-start | bytes 786440 | tf_op jit(solution)/shard_map/ppermute | solution.py:201
  124.5 12.3 %all-to-all-start.6 = ((f32[32,1,128]{2,1,0:T(1,128)}), f32[32,1,128]{2,1,0:T(1,128)S(1)}, u32[]{:S(2)}, u32[]{:S(2)}) async-start(f32[32,1,128]{2,1,0:T(1,128)} %get-tuple-element.34), calls=%async_computation.6 | async-start | bytes 32768 | tf_op jit(solution)/shard_map/all_to_all | solution.py:311
where the time goes:
time: 138 us
  blocking collectives  70.1 us (51%)
  starting transfers between devices  48.6 us (35%)
  waiting for transfers between devices  11.3 us (8%)
  Pallas kernels  7.36 us (5%)
    all_to_all x5, blocking collectives, exchange(): lax.all_to_all(value, axes, 0, 0, tiled=True, axis_index_groups=groups)  70.1 us
    ppermute x6, starting transfers between devices, passed(): return lax.ppermute(piece, axis, [(i, (i + d) % n) for i in range(n)])  31.5 us
    all_to_all x2, starting transfers between devices, exchange(): lax.all_to_all(value, axes, 0, 0, tiled=True, axis_index_groups=groups)  17.1 us
    ppermute x6, waiting for transfers between devices, passed(): return lax.ppermute(piece, axis, [(i, (i + d) % n) for i in range(n)])  7.51 us
    pallas_call x8, Pallas kernels, call(): pl.pallas_call(kernel, out_shape=outs, in_specs=[VMEM] * len(args), out_s...  4.08 us
    all_to_all x2, waiting for transfers between devices, exchange(): lax.all_to_all(value, axes, 0, 0, tiled=True, axis_index_groups=groups)  3.8 us
    pallas_call x2, Pallas kernels, deal(): pl.pallas_call(body, out_shape=[one] * m + list(extra_outs), in_specs=[HB...  3.28 us
  transfers between devices with their start and end apart: 8, of which 3 were waited for; matrix products, arithmetic and copies ran while one was open for 0% of the time, Pallas kernels for 1%

commit v1 on v0

--- a/solution.py
+++ b/solution.py
@@ -11,7 +11,6 @@
 HALF = 64
 CAP = 4
 GROUP = 8
-PIECES = 1
 PARAMS = pltpu.CompilerParams(vmem_limit_bytes=16 * 1024 * 1024)
 FIRST = {"z": lambda n: 13, "c": lambda n: n - 1, "y": lambda n: n // 2, "x": lambda n: n // 2}
 STEP = {"z": 1, "c": 1, "y": 1, "x": 1}
@@ -75,19 +74,15 @@
 
 def slice_copies(sources, outs, shifts, sems):
     x = lax.axis_index("x")
-    copies = []
-    for d, out in zip(shifts, outs):
-        for i, source in enumerate(sources):
-            at = lax.rem(x + d, source.shape[0])
-            rows = source.shape[1] // PIECES
-            for k in range(PIECES):
-                part = pl.ds(k * rows, rows)
-                copies.append(
-                    pltpu.make_async_copy(
-                        source.at[at, part, :], out.at[i, part, :], sems.at[len(copies)]
-                    )
-                )
-    return copies
+    return [
+        pltpu.make_async_copy(
+            source.at[lax.rem(x + d, source.shape[0])],
+            out.at[i],
+            sems.at[j * len(sources) + i],
+        )
+        for j, (d, out) in enumerate(zip(shifts, outs))
+        for i, source in enumerate(sources)
+    ]
 
 
 def deal(arrays, shifts, kernel=None, extra=(), extra_outs=()):
@@ -116,7 +111,7 @@
         in_specs=[HBM] * (n + k),
         out_specs=[VMEM] * (m + len(extra_outs)),
         scratch_shapes=[pltpu.VMEM(a.shape, a.dtype) for a in extra]
-        + [pltpu.SemaphoreType.DMA((m * n * PIECES,)), pltpu.SemaphoreType.DMA((max(k, 1),))],
+        + [pltpu.SemaphoreType.DMA((m * n,)), pltpu.SemaphoreType.DMA((max(k, 1),))],
         compiler_params=PARAMS,
     )(*[in_hbm(a) for a in (*arrays, *extra)])
 
@@ -157,9 +152,10 @@
         sel_ref[q] = ones_where(lane == at)
 
 
-def slot_scales(ids, weights_ref, scale_ref):
+def scale_kernel(routes_ref, weights_ref, gain_ref, scale_ref, last_ref):
     z, c, x = lax.axis_index("z"), lax.axis_index("c"), lax.axis_index("x")
-    chips = ids[0].shape[0]
+    chips = routes_ref.shape[0]
+    ids = [routes_ref[:, k, :] for k in range(CAP)]
     own = z * GROUP + c * CAP + x
     hit = named(ids, own)
     rank = dot(hit.astype(BF), earlier())
@@ -173,6 +169,7 @@
             value = jnp.sum(jnp.where(at, weight, 0.0), axis=1, keepdims=True)
             start = (i * CAP + q) * chips
             scale_ref[start : start + chips, :] = jnp.broadcast_to(value, (chips, LANES))
+    last_ref[...] = jnp.broadcast_to(gain_ref[...], last_ref.shape)
 
 
 def three_rows(gain, tail_ref):
@@ -184,25 +181,16 @@
     tail_ref[...] = tail.astype(BF)
 
 
-def routing_kernel(
-    routes_ref, weights_ref, tok_ref, gain_ref, last_ref,
-    out_ref, place_ref, sel_ref, tail_ref, scale_ref, last_out_ref,
-):
+def routing_kernel(routes_ref, tok_ref, gain_ref, out_ref, place_ref, sel_ref, tail_ref):
     ids = [routes_ref[:, k, :] for k in range(CAP)]
     dispatch(ids, tok_ref, out_ref, place_ref)
     select_table(ids, sel_ref)
     three_rows(gain_ref[...], tail_ref)
-    slot_scales(ids, weights_ref, scale_ref)
-    last_out_ref[...] = jnp.broadcast_to(last_ref[...], last_out_ref.shape)
 
 
 def passed(piece, d, axis):
     n = lax.axis_size(axis)
     return lax.ppermute(piece, axis, [(i, (i + d) % n) for i in range(n)])
-
-
-def mark_kernel(in_ref, out_ref):
-    out_ref[...] = in_ref[...]
 
 
 def select_kernel(recv_ref, sel_ref, tail_ref, out_ref):
@@ -255,17 +243,25 @@
         out_ref[y] = act
 
 
-def down_kernel(act_ref, scale_ref, *refs):
-    *weights, out_ref = refs
-    n = len(weights)
-    x = lax.axis_index("x")
+def slot_rows(act_ref):
     rows = act_ref.shape[0] // len(GATHER)
     at = [GATHER.index(y) * rows for y in REDUCE]
-    act = jnp.concatenate([act_ref[i : i + rows, :] for i in at], axis=0)
+    return jnp.concatenate([act_ref[i : i + rows, :] for i in at], axis=0)
+
+
+def own_down_kernel(act_ref, scale_ref, weight_ref, out_ref):
+    out_ref[...] = (dot(slot_rows(act_ref), weight_ref[0]) * scale_ref[...]).astype(BF)
+
+
+def down_kernel(act_ref, scale_ref, own_ref, *refs):
+    *weights, out_ref = refs
+    n = len(weights) + 1
+    x = lax.axis_index("x")
+    act = slot_rows(act_ref)
     scale = scale_ref[...]
     for d in range(n):
         at = place_of(x - d + n, "x")
-        out = (dot(act, weights[d][0]) * scale).astype(BF)
+        out = (dot(act, weights[d - 1][0]) * scale).astype(BF) if d else own_ref[...]
         out_ref[at] = out[0:64]
         out_ref[n + at] = out[64:128]
 
@@ -320,18 +316,16 @@
     weights = jnp.transpose(route_weights.reshape(chips, LANES, CAP), (0, 2, 1))
 
     square = shape((LANES, LANES), BF)
-    own, near, far, back, outgoing, place, sel, tail, scale, last_gain = deal(
+    own, near, far, back, outgoing, place, sel, tail = deal(
         [w_gate, w_up],
         [0, 1, 2, 3],
         routing_kernel,
-        (routes, weights, tokens, in_gain.reshape(1, local), out_gain.reshape(1, local)),
+        (routes, tokens, in_gain.reshape(1, local)),
         (
             square,
             square,
             shape((CAP, LANES, LANES), BF),
             shape((8, LANES), BF),
-            shape((LANES, LANES), F32),
-            shape((8, LANES), F32),
         ),
     )
     gate_up = [own, passed(near, 1, "x"), passed(far, 2, "x"), passed(back, 3, "x")]
@@ -343,11 +337,19 @@
     )
     slots = exchange(slots, ("c", "x"))
     parts = call(gate_up_kernel, shape((LANES, 2 * hidden + LANES), BF), slots, *gate_up)
-    last_gain = call(mark_kernel, shape((8, LANES), F32), last_gain)
+    scale, last_gain = call(
+        scale_kernel,
+        [shape((LANES, LANES), F32), shape((8, LANES), F32)],
+        routes,
+        weights,
+        out_gain.reshape(1, local),
+    )
     parts = exchange(parts.reshape(ys, LANES // ys, 2 * hidden + LANES), ("y",), REDUCE)
     act = call(lambda *refs: act_kernel(width, *refs), shape((ys, LANES // ys, hidden), BF), parts)
     act = exchange(act, ("y",), GATHER).reshape(LANES, hidden)
-    answers = call(down_kernel, shape((GROUP, 64, LANES), BF), act, scale, *down)
+    own, *others = down
+    own = call(own_down_kernel, shape((LANES, LANES), BF), act, scale, own)
+    answers = call(down_kernel, shape((GROUP, 64, LANES), BF), act, scale, own, *others)
     answers = exchange(answers, ("c", "x"))
     mixed = call(combine_kernel, shape((LANES, local), BF), answers, sel)
     returned = exchange(mixed.reshape(chips, GROUP, local), ("z",))

time: 138 us -> 137 us (level)
  blocking collectives: 70.1 us -> 82.3 us
  starting transfers between devices: 48.6 us -> 40.1 us
  waiting for transfers between devices: 11.3 us -> 6.36 us
    all_to_all x5 -> x6, blocking collectives: 70.1 us -> 82.3 us  [exchange(): lax.all_to_all(value, axes, 0, 0, tiled=True, axis_index_groups=groups)]
    all_to_all x2 -> x1, starting transfers between devices: 17.1 us -> 8.65 us  [exchange(): lax.all_to_all(value, axes, 0, 0, tiled=True, axis_index_groups=groups)]
    all_to_all x2 -> x1, waiting for transfers between devices: 3.8 us -> 0.01 us  [exchange(): lax.all_to_all(value, axes, 0, 0, tiled=True, axis_index_groups=groups)]
    pallas_call x8 -> x9, Pallas kernels: 4.08 us -> 3.85 us  [call(): pl.pallas_call(kernel, out_shape=outs, in_specs=[VMEM] * len(args), out_s...]
  transfers between devices with their start and end apart: 8 -> 7, of which waited for: 3 -> 2; matrix products, arithmetic and copies ran while one was open for 0% -> 0% of each run, Pallas kernels for 1% -> 1%
where the time goes in v1:
time: 137 us
  blocking collectives  82.3 us (60%)
  starting transfers between devices  40.1 us (29%)
  Pallas kernels  7.09 us (5%)
  waiting for transfers between devices  6.36 us (5%)
    all_to_all x6, blocking collectives, exchange(): lax.all_to_all(value, axes, 0, 0, tiled=True, axis_index_groups=groups)  82.3 us
    ppermute x6, starting transfers between devices, passed(): return lax.ppermute(piece, axis, [(i, (i + d) % n) for i in range(n)])  31.5 us
    all_to_all x1, starting transfers between devices, exchange(): lax.all_to_all(value, axes, 0, 0, tiled=True, axis_index_groups=groups)  8.65 us
    ppermute x6, waiting for transfers between devices, passed(): return lax.ppermute(piece, axis, [(i, (i + d) % n) for i in range(n)])  6.36 us
    pallas_call x9, Pallas kernels, call(): pl.pallas_call(kernel, out_shape=outs, in_specs=[VMEM] * len(args), out_s...  3.85 us
    pallas_call x2, Pallas kernels, deal(): pl.pallas_call(body, out_shape=[one] * m + list(extra_outs), in_specs=[HB...  3.24 us
  transfers between devices with their start and end apart: 7, of which 2 were waited for; matrix products, arithmetic and copies ran while one was open for 0% of the time, Pallas kernels for 1%

profile of v1, /device:TPU:2, one launch (start us, length us, event | category | flops | bytes accessed | tf_op | source)
XLA Modules:
  0.0 136.7 jit_solution(17955169046215666086)
XLA Ops:
  0.0 2.0 %shard_map.82 = (bf16[2,128,1024]{2,1,0:T(8,128)(2,1)S(1)}, bf16[2,128,1024]{2,1,0:T(8,128)(2,1)S(1)}, bf16[2,128,1024]{2,1,0:T(8,128)(2,1)S(1)}, bf16[2,128,102...) custom-call(bf16[4,128,1024]{2,1,0:T(8,128)(2,1)} %refs_0_.2, ...), custom_call_target="tpu_custom_call" | custom-call | tf_op jit(solution)/shard_map/pallas_call | solution.py:108
  2.0 3.4 %collective-permute-start = (bf16[2,128,1024]{2,1,0:T(8,128)(2,1)S(1)}, bf16[2,128,1024]{2,1,0:T(8,128)(2,1)S(1)}, u32[]{:S(2)}, u32[]{:S(2)}) collective-permute-start(bf16[2,128,1024]{2,1,0:T(8,128)(2,1)S(1)} %get-tuple-element.25), channel_id=1, source_target_pairs={{0,1},{1,2},{2,3},{3,0},{4,5},{5,6},{6,7},{7,4},{8,9},{9,10},{10,1... | collective-permute-start | bytes 1572872 | tf_op jit(solution)/shard_map/ppermute | solution.py:193
  5.5 15.6 %collective-permute-start.1 = (bf16[2,128,1024]{2,1,0:T(8,128)(2,1)S(1)}, bf16[2,128,1024]{2,1,0:T(8,128)(2,1)S(1)}, u32[]{:S(2)}, u32[]{:S(2)}) collective-permute-start(bf16[2,128,1024]{2,1,0:T(8,128)(2,1)S(1)} %get-tuple-element.26), channel_id=1, source_target_pairs={{0,2},{1,3},{2,0},{3,1},{4,6},{5,7},{6,4},{7,5},{8,10},{9,11},{10,... | collective-permute-start | bytes 1572872 | tf_op jit(solution)/shard_map/ppermute | solution.py:193
  21.0 1.9 %collective-permute-start.2 = (bf16[2,128,1024]{2,1,0:T(8,128)(2,1)S(1)}, bf16[2,128,1024]{2,1,0:T(8,128)(2,1)S(1)}, u32[]{:S(2)}, u32[]{:S(2)}) collective-permute-start(bf16[2,128,1024]{2,1,0:T(8,128)(2,1)S(1)} %get-tuple-element.27), channel_id=1, source_target_pairs={{0,3},{1,0},{2,1},{3,2},{4,7},{5,4},{6,5},{7,6},{8,11},{9,8},{10,9... | collective-permute-start | bytes 1572872 | tf_op jit(solution)/shard_map/ppermute | solution.py:193
  23.0 17.9 %all_to_all.35 = bf16[16,8,128]{2,1,0:T(8,128)(2,1)S(1)} all-to-all(bf16[16,8,128]{2,1,0:T(8,128)(2,1)S(1)} %bitcast.23), channel_id=1, replica_groups={{832,896,960,0,64,128,192,256,320,384,448,512,576,640,704,768},{833,897..., dimensions={0} | all-to-all | bytes 65536 | tf_op jit(solution)/shard_map/all_to_all | solution.py:307
  40.9 0.2 shard_map.83
  41.1 8.6 %all_to_all.36.rows_ref = bf16[8,72,128]{2,1,0:T(8,128)(2,1)S(1)} all-to-all(bf16[8,72,128]{2,1,0:T(8,128)(2,1)S(1)} %shard_map.83), channel_id=1, replica_groups={{34,35,32,33,2,3,0,1},{38,39,36,37,6,7,4,5},{42,43,40,41,10,11,8,9},{46..., dimensions={0} | all-to-all | bytes 294912 | tf_op jit(solution)/shard_map/all_to_all | solution.py:307
  49.6 0.0 collective-permute-done.refs_1_
  49.6 0.0 collective-permute-done.1.refs_2_
  49.6 0.0 collective-permute-done.2.refs_3_
  49.6 0.7 shard_map.84
  50.3 21.1 %all_to_all.37.refs_0_ = bf16[8,16,2176]{2,1,0:T(8,128)(2,1)S(1)} all-to-all(bf16[8,16,2176]{2,1,0:T(8,128)(2,1)S(1)} %bitcast.16), channel_id=1, replica_groups={{16,28,8,20,0,12,24,4},{17,29,9,21,1,13,25,5},{18,30,10,22,2,14,26,6},{..., dimensions={0} | all-to-all | bytes 1114112 | tf_op jit(solution)/shard_map/all_to_all | solution.py:307
  71.4 0.9 shard_map.85
  72.3 8.6 %all-to-all-start.3 = ((bf16[8,16,1024]{2,1,0:T(8,128)(2,1)}), bf16[8,16,1024]{2,1,0:T(8,128)(2,1)S(1)}, u32[]{:S(2)}, u32[]{:S(2)}) async-start(bf16[8,16,1024]{2,1,0:T(8,128)(2,1)} %shard_map.85), calls=%async_computation.3 | async-start | bytes 524288 | tf_op jit(solution)/shard_map/all_to_all | solution.py:307
  80.9 0.0 copy-start
  80.9 0.0 copy-start.1
  80.9 1.2 shard_map.87
  82.2 3.3 %collective-permute-start.3 = (bf16[1,1024,128]{2,1,0:T(8,128)(2,1)S(1)}, bf16[1,1024,128]{2,1,0:T(8,128)(2,1)S(1)}, u32[]{:S(2)}, u32[]{:S(2)}) collective-permute-start(bf16[1,1024,128]{2,1,0:T(8,128)(2,1)S(1)} %get-tuple-element.30), channel_id=1, source_target_pairs={{0,1},{1,2},{2,3},{3,0},{4,5},{5,6},{6,7},{7,4},{8,9},{9,10},{10,1... | collective-permute-start | bytes 786440 | tf_op jit(solution)/shard_map/ppermute | solution.py:193
  85.4 3.0 %collective-permute-start.4 = (bf16[1,1024,128]{2,1,0:T(8,128)(2,1)S(1)}, bf16[1,1024,128]{2,1,0:T(8,128)(2,1)S(1)}, u32[]{:S(2)}, u32[]{:S(2)}) collective-permute-start(bf16[1,1024,128]{2,1,0:T(8,128)(2,1)S(1)} %get-tuple-element.31), channel_id=1, source_target_pairs={{0,2},{1,3},{2,0},{3,1},{4,6},{5,7},{6,4},{7,5},{8,10},{9,11},{10,... | collective-permute-start | bytes 786440 | tf_op jit(solution)/shard_map/ppermute | solution.py:193
  88.5 4.3 %collective-permute-start.5 = (bf16[1,1024,128]{2,1,0:T(8,128)(2,1)S(1)}, bf16[1,1024,128]{2,1,0:T(8,128)(2,1)S(1)}, u32[]{:S(2)}, u32[]{:S(2)}) collective-permute-start(bf16[1,1024,128]{2,1,0:T(8,128)(2,1)S(1)} %get-tuple-element.32), channel_id=1, source_target_pairs={{0,3},{1,0},{2,1},{3,2},{4,7},{5,4},{6,5},{7,6},{8,11},{9,8},{10,9... | collective-permute-start | bytes 786440 | tf_op jit(solution)/shard_map/ppermute | solution.py:193
  92.7 0.0 copy-start.2
  92.7 0.0 copy-done
  92.8 0.0 copy-done.1
  92.8 0.6 copy-done.2
  93.4 0.2 shard_map.86
  93.6 0.0 all-to-all-done.3
  93.7 0.2 shard_map.88.own_ref
  93.9 0.0 collective-permute-done.3.refs_0_
  93.9 3.6 %collective-permute-done.4.refs_1_ = bf16[1,1024,128]{2,1,0:T(8,128)(2,1)S(1)} collective-permute-done((bf16[1,1024,128]{2,1,0:T(8,128)(2,1)S(1)}, bf16[1,1024,128]{2,1,0:T(8,128)(2,1)S(1)}, u32[]{:S(2)}, u32[]{:S(2)}) %collective-permute-start.4) | collective-permute-done | bytes 262176 | tf_op jit(solution)/shard_map/ppermute | solution.py:193
  97.5 2.7 %collective-permute-done.5.refs_2_ = bf16[1,1024,128]{2,1,0:T(8,128)(2,1)S(1)} collective-permute-done((bf16[1,1024,128]{2,1,0:T(8,128)(2,1)S(1)}, bf16[1,1024,128]{2,1,0:T(8,128)(2,1)S(1)}, u32[]{:S(2)}, u32[]{:S(2)}) %collective-permute-start.5) | collective-permute-done | bytes 262176 | tf_op jit(solution)/shard_map/ppermute | solution.py:193
  100.2 0.4 shard_map.89
  100.6 7.7 %all_to_all.38.parts_ref = bf16[8,64,128]{2,1,0:T(8,128)(2,1)S(1)} all-to-all(bf16[8,64,128]{2,1,0:T(8,128)(2,1)S(1)} %shard_map.89), channel_id=1, replica_groups={{34,35,32,33,2,3,0,1},{38,39,36,37,6,7,4,5},{42,43,40,41,10,11,8,9},{46..., dimensions={0} | all-to-all | bytes 262144 | tf_op jit(solution)/shard_map/all_to_all | solution.py:307
  108.3 0.2 shard_map.90
  108.5 15.0 %all_to_all.39 = bf16[16,8,128]{2,1,0:T(8,128)(2,1)S(1)} all-to-all(bf16[16,8,128]{2,1,0:T(8,128)(2,1)S(1)} %bitcast.20), channel_id=1, replica_groups={{832,896,960,0,64,128,192,256,320,384,448,512,576,640,704,768},{833,897..., dimensions={0} | all-to-all | bytes 65536 | tf_op jit(solution)/shard_map/all_to_all | solution.py:307
  123.5 0.3 shard_map.91
  123.8 12.1 %all_to_all.40.refs_0_ = f32[32,1,128]{2,1,0:T(1,128)S(1)} all-to-all(f32[32,1,128]{2,1,0:T(1,128)S(1)} %get-tuple-element.34), channel_id=1, replica_groups={{18,19,16,17,22,23,20,21,26,27,24,25,30,31,28,29,2,3,0,1,6,7,4,5,10,11,..., dimensions={0} | all-to-all | bytes 32768 | tf_op jit(solution)/shard_map/all_to_all | solution.py:307
  135.9 0.8 shard_map.92
Async XLA Ops:
  2.0 47.6 %collective-permute-start = (bf16[2,128,1024]{2,1,0:T(8,128)(2,1)S(1)}, bf16[2,128,1024]{2,1,0:T(8,128)(2,1)S(1)}, u32[]{:S(2)}, u32[]{:S(2)}) collective-permute-start(bf16[2,128,1024]{2,1,0:T(8,128)(2,1)S(1)} %get-tuple-element.25), channel_id=1, source_target_pairs={{0,1},{1,2},{2,3},{3,0},{4,5},{5,6},{6,7},{7,4},{8,9},{9,10},{10,1... | collective-permute-start | bytes 1572872 | tf_op jit(solution)/shard_map/ppermute | solution.py:193
  5.5 44.2 %collective-permute-start.1 = (bf16[2,128,1024]{2,1,0:T(8,128)(2,1)S(1)}, bf16[2,128,1024]{2,1,0:T(8,128)(2,1)S(1)}, u32[]{:S(2)}, u32[]{:S(2)}) collective-permute-start(bf16[2,128,1024]{2,1,0:T(8,128)(2,1)S(1)} %get-tuple-element.26), channel_id=1, source_target_pairs={{0,2},{1,3},{2,0},{3,1},{4,6},{5,7},{6,4},{7,5},{8,10},{9,11},{10,... | collective-permute-start | bytes 1572872 | tf_op jit(solution)/shard_map/ppermute | solution.py:193
  21.0 28.6 %collective-permute-start.2 = (bf16[2,128,1024]{2,1,0:T(8,128)(2,1)S(1)}, bf16[2,128,1024]{2,1,0:T(8,128)(2,1)S(1)}, u32[]{:S(2)}, u32[]{:S(2)}) collective-permute-start(bf16[2,128,1024]{2,1,0:T(8,128)(2,1)S(1)} %get-tuple-element.27), channel_id=1, source_target_pairs={{0,3},{1,0},{2,1},{3,2},{4,7},{5,4},{6,5},{7,6},{8,11},{9,8},{10,9... | collective-permute-start | bytes 1572872 | tf_op jit(solution)/shard_map/ppermute | solution.py:193
  72.3 21.4 %all-to-all-start.3 = ((bf16[8,16,1024]{2,1,0:T(8,128)(2,1)}), bf16[8,16,1024]{2,1,0:T(8,128)(2,1)S(1)}, u32[]{:S(2)}, u32[]{:S(2)}) async-start(bf16[8,16,1024]{2,1,0:T(8,128)(2,1)} %shard_map.85), calls=%async_computation.3 | async-start | bytes 524288 | tf_op jit(solution)/shard_map/all_to_all | solution.py:307
  80.9 11.8 %copy-start = (s32[2048,4]{0,1:T(4,128)S(1)}, s32[2048,4]{0,1:T(4,128)}, u32[]{:S(2)}) copy-start(s32[2048,4]{0,1:T(4,128)} %param.11) | copy-start | bytes 98308
  80.9 11.8 %copy-start.1 = (f32[2048,4]{0,1:T(4,128)S(1)}, f32[2048,4]{0,1:T(4,128)}, u32[]{:S(2)}) copy-start(f32[2048,4]{0,1:T(4,128)} %param.12) | copy-start | bytes 98308
  82.2 11.7 %collective-permute-start.3 = (bf16[1,1024,128]{2,1,0:T(8,128)(2,1)S(1)}, bf16[1,1024,128]{2,1,0:T(8,128)(2,1)S(1)}, u32[]{:S(2)}, u32[]{:S(2)}) collective-permute-start(bf16[1,1024,128]{2,1,0:T(8,128)(2,1)S(1)} %get-tuple-element.30), channel_id=1, source_target_pairs={{0,1},{1,2},{2,3},{3,0},{4,5},{5,6},{6,7},{7,4},{8,9},{9,10},{10,1... | collective-permute-start | bytes 786440 | tf_op jit(solution)/shard_map/ppermute | solution.py:193
  85.4 12.1 %collective-permute-start.4 = (bf16[1,1024,128]{2,1,0:T(8,128)(2,1)S(1)}, bf16[1,1024,128]{2,1,0:T(8,128)(2,1)S(1)}, u32[]{:S(2)}, u32[]{:S(2)}) collective-permute-start(bf16[1,1024,128]{2,1,0:T(8,128)(2,1)S(1)} %get-tuple-element.31), channel_id=1, source_target_pairs={{0,2},{1,3},{2,0},{3,1},{4,6},{5,7},{6,4},{7,5},{8,10},{9,11},{10,... | collective-permute-start | bytes 786440 | tf_op jit(solution)/shard_map/ppermute | solution.py:193
  88.5 11.8 %collective-permute-start.5 = (bf16[1,1024,128]{2,1,0:T(8,128)(2,1)S(1)}, bf16[1,1024,128]{2,1,0:T(8,128)(2,1)S(1)}, u32[]{:S(2)}, u32[]{:S(2)}) collective-permute-start(bf16[1,1024,128]{2,1,0:T(8,128)(2,1)S(1)} %get-tuple-element.32), channel_id=1, source_target_pairs={{0,3},{1,0},{2,1},{3,2},{4,7},{5,4},{6,5},{7,6},{8,11},{9,8},{10,9... | collective-permute-start | bytes 786440 | tf_op jit(solution)/shard_map/ppermute | solution.py:193
  92.7 0.7 copy-start.2

commit v2 on v1

--- a/solution.py
+++ b/solution.py
@@ -222,31 +222,59 @@
         lhs = (raw * gain).astype(BF)
         gate = gate + dot(lhs, weights[d][0])
         up = up + dot(lhs, weights[d][1])
-    out_ref[:, 0:hidden] = gate.astype(BF)
-    out_ref[:, hidden : 2 * hidden] = up.astype(BF)
+    ys = out_ref.shape[0]
+    share, blocks = LANES // ys, hidden // LANES
+    for i, total in enumerate((gate, up)):
+        total = total.astype(BF)
+        for j in range(blocks):
+            part = total[:, j * LANES : (j + 1) * LANES]
+            at = (i * blocks + j) * share
+            for y in range(ys):
+                out_ref[y, at : at + share, :] = part[y * share : (y + 1) * share]
     high = squares.astype(BF).astype(F32)
-    lane = iota((LANES, LANES), 1)
-    out_ref[:, 2 * hidden :] = jnp.where(lane < HALF, high, squares - high).astype(BF)
+    low = squares - high
+    lane = iota((8, LANES), 1)
+    for y in range(ys):
+        start = y * share
+        first, second = slice(start, start + 8), slice(start + 8, start + 16)
+        out_ref[y, 2 * blocks * share :, :] = jnp.where(
+            lane < 32,
+            high[first],
+            jnp.where(lane < 64, low[first], jnp.where(lane < 96, high[second], low[second])),
+        ).astype(BF)
 
 
 def act_kernel(width, parts_ref, out_ref):
+    ys, rows, _ = parts_ref.shape
     total = parts_ref[0].astype(F32)
-    for y in range(1, parts_ref.shape[0]):
+    for y in range(1, ys):
         total = total + parts_ref[y].astype(F32)
-    hidden = out_ref.shape[2]
-    squares = total[:, 2 * hidden : 2 * hidden + 1] + total[:, 2 * hidden + HALF : 2 * hidden + HALF + 1]
+    share = out_ref.shape[1] // ((rows - 8) // (2 * 16))
+    tail = total[rows - 8 :]
+    squares = jnp.concatenate(
+        [tail[:, 0:1] + tail[:, 32:33], tail[:, 64:65] + tail[:, 96:97]], axis=0
+    )
     scale = lax.rsqrt(squares / width + EPS)
-    gate = total[:, 0:hidden] * scale
-    up = total[:, hidden : 2 * hidden] * scale
-    act = (gate / (1.0 + jnp.exp(-gate)) * up).astype(BF)
-    for y in range(out_ref.shape[0]):
-        out_ref[y] = act
+    half = (rows - 8) // 2
+    for j in range(half // share):
+        gate = total[j * share : (j + 1) * share] * scale
+        up = total[half + j * share : half + (j + 1) * share] * scale
+        act = (gate / (1.0 + jnp.exp(-gate)) * up).astype(BF)
+        for y in range(ys):
+            out_ref[y, j * share : (j + 1) * share, :] = act
 
 
 def slot_rows(act_ref):
-    rows = act_ref.shape[0] // len(GATHER)
-    at = [GATHER.index(y) * rows for y in REDUCE]
-    return jnp.concatenate([act_ref[i : i + rows, :] for i in at], axis=0)
+    ys, rows, _ = act_ref.shape
+    share = LANES // ys
+    at = [GATHER.index(y) for y in REDUCE]
+    return jnp.concatenate(
+        [
+            jnp.concatenate([act_ref[i, j : j + share, :] for i in at], axis=0)
+            for j in range(0, rows, share)
+        ],
+        axis=1,
+    )
 
 
 def own_down_kernel(act_ref, scale_ref, weight_ref, out_ref):
@@ -336,7 +364,10 @@
         select_kernel, shape((GROUP, 72, LANES), BF), arrived.reshape(LANES, local), sel, tail
     )
     slots = exchange(slots, ("c", "x"))
-    parts = call(gate_up_kernel, shape((LANES, 2 * hidden + LANES), BF), slots, *gate_up)
+    share = LANES // ys
+    parts = call(
+        gate_up_kernel, shape((ys, 2 * hidden // LANES * share + 8, LANES), BF), slots, *gate_up
+    )
     scale, last_gain = call(
         scale_kernel,
         [shape((LANES, LANES), F32), shape((8, LANES), F32)],
@@ -344,9 +375,13 @@
         weights,
         out_gain.reshape(1, local),
     )
-    parts = exchange(parts.reshape(ys, LANES // ys, 2 * hidden + LANES), ("y",), REDUCE)
-    act = call(lambda *refs: act_kernel(width, *refs), shape((ys, LANES // ys, hidden), BF), parts)
-    act = exchange(act, ("y",), GATHER).reshape(LANES, hidden)
+    parts = exchange(parts, ("y",), REDUCE)
+    act = call(
+        lambda *refs: act_kernel(width, *refs),
+        shape((ys, hidden // LANES * share, LANES), BF),
+        parts,
+    )
+    act = exchange(act, ("y",), GATHER)
     own, *others = down
     own = call(own_down_kernel, shape((LANES, LANES), BF), act, scale, own)
     answers = call(down_kernel, shape((GROUP, 64, LANES), BF), act, scale, own, *others)

time: 137 us -> 137 us (level)
  no operation moved by 1% of the time
where the time goes in v2:
time: 137 us; the launch traced here: 136 us
  blocking collectives  82.1 us (60%)
  starting transfers between devices  40.1 us (29%)
  Pallas kernels  7.16 us (5%)
  waiting for transfers between devices  6.35 us (5%)
    all_to_all x6, blocking collectives, exchange(): lax.all_to_all(value, axes, 0, 0, tiled=True, axis_index_groups=groups)  82.1 us
    ppermute x6, starting transfers between devices, passed(): return lax.ppermute(piece, axis, [(i, (i + d) % n) for i in range(n)])  31.5 us
    all_to_all x1, starting transfers between devices, exchange(): lax.all_to_all(value, axes, 0, 0, tiled=True, axis_index_groups=groups)  8.67 us
    ppermute x6, waiting for transfers between devices, passed(): return lax.ppermute(piece, axis, [(i, (i + d) % n) for i in range(n)])  6.34 us
    pallas_call x9, Pallas kernels, call(): pl.pallas_call(kernel, out_shape=outs, in_specs=[VMEM] * len(args), out_s...  3.92 us
    pallas_call x2, Pallas kernels, deal(): pl.pallas_call(body, out_shape=[one] * m + list(extra_outs), in_specs=[HB...  3.24 us
  transfers between devices with their start and end apart: 7, of which 2 were waited for; matrix products, arithmetic and copies ran while one was open for 0% of the time, Pallas kernels for 1%

profile of v2, /device:TPU:2, one launch (start us, length us, event | category | flops | bytes accessed | tf_op | source)
XLA Modules:
  0.0 136.5 jit_solution(14336864252678741841)
XLA Ops:
  0.0 2.0 %shard_map.82 = (bf16[2,128,1024]{2,1,0:T(8,128)(2,1)S(1)}, bf16[2,128,1024]{2,1,0:T(8,128)(2,1)S(1)}, bf16[2,128,1024]{2,1,0:T(8,128)(2,1)S(1)}, bf16[2,128,102...) custom-call(bf16[4,128,1024]{2,1,0:T(8,128)(2,1)} %refs_0_.2, ...), custom_call_target="tpu_custom_call" | custom-call | tf_op jit(solution)/shard_map/pallas_call | solution.py:108
  2.0 3.4 %collective-permute-start = (bf16[2,128,1024]{2,1,0:T(8,128)(2,1)S(1)}, bf16[2,128,1024]{2,1,0:T(8,128)(2,1)S(1)}, u32[]{:S(2)}, u32[]{:S(2)}) collective-permute-start(bf16[2,128,1024]{2,1,0:T(8,128)(2,1)S(1)} %get-tuple-element.25), channel_id=1, source_target_pairs={{0,1},{1,2},{2,3},{3,0},{4,5},{5,6},{6,7},{7,4},{8,9},{9,10},{10,1... | collective-permute-start | bytes 1572872 | tf_op jit(solution)/shard_map/ppermute | solution.py:193
  5.5 15.6 %collective-permute-start.1 = (bf16[2,128,1024]{2,1,0:T(8,128)(2,1)S(1)}, bf16[2,128,1024]{2,1,0:T(8,128)(2,1)S(1)}, u32[]{:S(2)}, u32[]{:S(2)}) collective-permute-start(bf16[2,128,1024]{2,1,0:T(8,128)(2,1)S(1)} %get-tuple-element.26), channel_id=1, source_target_pairs={{0,2},{1,3},{2,0},{3,1},{4,6},{5,7},{6,4},{7,5},{8,10},{9,11},{10,... | collective-permute-start | bytes 1572872 | tf_op jit(solution)/shard_map/ppermute | solution.py:193
  21.0 1.9 %collective-permute-start.2 = (bf16[2,128,1024]{2,1,0:T(8,128)(2,1)S(1)}, bf16[2,128,1024]{2,1,0:T(8,128)(2,1)S(1)}, u32[]{:S(2)}, u32[]{:S(2)}) collective-permute-start(bf16[2,128,1024]{2,1,0:T(8,128)(2,1)S(1)} %get-tuple-element.27), channel_id=1, source_target_pairs={{0,3},{1,0},{2,1},{3,2},{4,7},{5,4},{6,5},{7,6},{8,11},{9,8},{10,9... | collective-permute-start | bytes 1572872 | tf_op jit(solution)/shard_map/ppermute | solution.py:193
  23.0 17.9 %all_to_all.35 = bf16[16,8,128]{2,1,0:T(8,128)(2,1)S(1)} all-to-all(bf16[16,8,128]{2,1,0:T(8,128)(2,1)S(1)} %bitcast.18), channel_id=1, replica_groups={{832,896,960,0,64,128,192,256,320,384,448,512,576,640,704,768},{833,897..., dimensions={0} | all-to-all | bytes 65536 | tf_op jit(solution)/shard_map/all_to_all | solution.py:335
  40.9 0.2 shard_map.83
  41.1 8.6 %all_to_all.36.rows_ref = bf16[8,72,128]{2,1,0:T(8,128)(2,1)S(1)} all-to-all(bf16[8,72,128]{2,1,0:T(8,128)(2,1)S(1)} %shard_map.83), channel_id=1, replica_groups={{34,35,32,33,2,3,0,1},{38,39,36,37,6,7,4,5},{42,43,40,41,10,11,8,9},{46..., dimensions={0} | all-to-all | bytes 294912 | tf_op jit(solution)/shard_map/all_to_all | solution.py:335
  49.6 0.0 collective-permute-done.refs_1_
  49.6 0.0 collective-permute-done.1.refs_2_
  49.6 0.0 collective-permute-done.2.refs_3_
  49.6 0.7 shard_map.84
  50.3 20.8 %all_to_all.37.refs_0_ = bf16[8,264,128]{2,1,0:T(8,128)(2,1)S(1)} all-to-all(bf16[8,264,128]{2,1,0:T(8,128)(2,1)S(1)} %shard_map.84), channel_id=1, replica_groups={{16,28,8,20,0,12,24,4},{17,29,9,21,1,13,25,5},{18,30,10,22,2,14,26,6},{..., dimensions={0} | all-to-all | bytes 1081344 | tf_op jit(solution)/shard_map/all_to_all | solution.py:335
  71.1 1.0 shard_map.85
  72.1 8.7 %all-to-all-start.3 = ((bf16[8,128,128]{2,1,0:T(8,128)(2,1)}), bf16[8,128,128]{2,1,0:T(8,128)(2,1)S(1)}, u32[]{:S(2)}, u32[]{:S(2)}) async-start(bf16[8,128,128]{2,1,0:T(8,128)(2,1)} %shard_map.85), calls=%async_computation.3 | async-start | bytes 524288 | tf_op jit(solution)/shard_map/all_to_all | solution.py:335
  80.7 0.0 copy-start
  80.7 0.0 copy-start.1
  80.7 1.2 shard_map.87
  82.0 3.3 %collective-permute-start.3 = (bf16[1,1024,128]{2,1,0:T(8,128)(2,1)S(1)}, bf16[1,1024,128]{2,1,0:T(8,128)(2,1)S(1)}, u32[]{:S(2)}, u32[]{:S(2)}) collective-permute-start(bf16[1,1024,128]{2,1,0:T(8,128)(2,1)S(1)} %get-tuple-element.30), channel_id=1, source_target_pairs={{0,1},{1,2},{2,3},{3,0},{4,5},{5,6},{6,7},{7,4},{8,9},{9,10},{10,1... | collective-permute-start | bytes 786440 | tf_op jit(solution)/shard_map/ppermute | solution.py:193
  85.2 3.0 %collective-permute-start.4 = (bf16[1,1024,128]{2,1,0:T(8,128)(2,1)S(1)}, bf16[1,1024,128]{2,1,0:T(8,128)(2,1)S(1)}, u32[]{:S(2)}, u32[]{:S(2)}) collective-permute-start(bf16[1,1024,128]{2,1,0:T(8,128)(2,1)S(1)} %get-tuple-element.31), channel_id=1, source_target_pairs={{0,2},{1,3},{2,0},{3,1},{4,6},{5,7},{6,4},{7,5},{8,10},{9,11},{10,... | collective-permute-start | bytes 786440 | tf_op jit(solution)/shard_map/ppermute | solution.py:193
  88.3 4.3 %collective-permute-start.5 = (bf16[1,1024,128]{2,1,0:T(8,128)(2,1)S(1)}, bf16[1,1024,128]{2,1,0:T(8,128)(2,1)S(1)}, u32[]{:S(2)}, u32[]{:S(2)}) collective-permute-start(bf16[1,1024,128]{2,1,0:T(8,128)(2,1)S(1)} %get-tuple-element.32), channel_id=1, source_target_pairs={{0,3},{1,0},{2,1},{3,2},{4,7},{5,4},{6,5},{7,6},{8,11},{9,8},{10,9... | collective-permute-start | bytes 786440 | tf_op jit(solution)/shard_map/ppermute | solution.py:193
  92.5 0.0 copy-start.2
  92.5 0.0 copy-done
  92.5 0.0 copy-done.1
  92.6 0.6 copy-done.2
  93.2 0.2 shard_map.86
  93.4 0.0 all-to-all-done.3.act_ref
  93.4 0.2 shard_map.88.own_ref
  93.7 0.0 collective-permute-done.3.refs_0_
  93.7 3.6 %collective-permute-done.4.refs_1_ = bf16[1,1024,128]{2,1,0:T(8,128)(2,1)S(1)} collective-permute-done((bf16[1,1024,128]{2,1,0:T(8,128)(2,1)S(1)}, bf16[1,1024,128]{2,1,0:T(8,128)(2,1)S(1)}, u32[]{:S(2)}, u32[]{:S(2)}) %collective-permute-start.4) | collective-permute-done | bytes 262176 | tf_op jit(solution)/shard_map/ppermute | solution.py:193
  97.3 2.7 %collective-permute-done.5.refs_2_ = bf16[1,1024,128]{2,1,0:T(8,128)(2,1)S(1)} collective-permute-done((bf16[1,1024,128]{2,1,0:T(8,128)(2,1)S(1)}, bf16[1,1024,128]{2,1,0:T(8,128)(2,1)S(1)}, u32[]{:S(2)}, u32[]{:S(2)}) %collective-permute-start.5) | collective-permute-done | bytes 262176 | tf_op jit(solution)/shard_map/ppermute | solution.py:193
  100.0 0.4 shard_map.89
  100.4 7.7 %all_to_all.38.parts_ref = bf16[8,64,128]{2,1,0:T(8,128)(2,1)S(1)} all-to-all(bf16[8,64,128]{2,1,0:T(8,128)(2,1)S(1)} %shard_map.89), channel_id=1, replica_groups={{34,35,32,33,2,3,0,1},{38,39,36,37,6,7,4,5},{42,43,40,41,10,11,8,9},{46..., dimensions={0} | all-to-all | bytes 262144 | tf_op jit(solution)/shard_map/all_to_all | solution.py:335
  108.1 0.2 shard_map.90
  108.3 15.0 %all_to_all.39 = bf16[16,8,128]{2,1,0:T(8,128)(2,1)S(1)} all-to-all(bf16[16,8,128]{2,1,0:T(8,128)(2,1)S(1)} %bitcast.15), channel_id=1, replica_groups={{832,896,960,0,64,128,192,256,320,384,448,512,576,640,704,768},{833,897..., dimensions={0} | all-to-all | bytes 65536 | tf_op jit(solution)/shard_map/all_to_all | solution.py:335
  123.3 0.3 shard_map.91
  123.6 12.1 %all_to_all.40.refs_0_ = f32[32,1,128]{2,1,0:T(1,128)S(1)} all-to-all(f32[32,1,128]{2,1,0:T(1,128)S(1)} %get-tuple-element.34), channel_id=1, replica_groups={{18,19,16,17,22,23,20,21,26,27,24,25,30,31,28,29,2,3,0,1,6,7,4,5,10,11,..., dimensions={0} | all-to-all | bytes 32768 | tf_op jit(solution)/shard_map/all_to_all | solution.py:335
  135.7 0.8 shard_map.92
Async XLA Ops:
  2.0 47.6 %collective-permute-start = (bf16[2,128,1024]{2,1,0:T(8,128)(2,1)S(1)}, bf16[2,128,1024]{2,1,0:T(8,128)(2,1)S(1)}, u32[]{:S(2)}, u32[]{:S(2)}) collective-permute-start(bf16[2,128,1024]{2,1,0:T(8,128)(2,1)S(1)} %get-tuple-element.25), channel_id=1, source_target_pairs={{0,1},{1,2},{2,3},{3,0},{4,5},{5,6},{6,7},{7,4},{8,9},{9,10},{10,1... | collective-permute-start | bytes 1572872 | tf_op jit(solution)/shard_map/ppermute | solution.py:193
  5.5 44.2 %collective-permute-start.1 = (bf16[2,128,1024]{2,1,0:T(8,128)(2,1)S(1)}, bf16[2,128,1024]{2,1,0:T(8,128)(2,1)S(1)}, u32[]{:S(2)}, u32[]{:S(2)}) collective-permute-start(bf16[2,128,1024]{2,1,0:T(8,128)(2,1)S(1)} %get-tuple-element.26), channel_id=1, source_target_pairs={{0,2},{1,3},{2,0},{3,1},{4,6},{5,7},{6,4},{7,5},{8,10},{9,11},{10,... | collective-permute-start | bytes 1572872 | tf_op jit(solution)/shard_map/ppermute | solution.py:193
  21.0 28.6 %collective-permute-start.2 = (bf16[2,128,1024]{2,1,0:T(8,128)(2,1)S(1)}, bf16[2,128,1024]{2,1,0:T(8,128)(2,1)S(1)}, u32[]{:S(2)}, u32[]{:S(2)}) collective-permute-start(bf16[2,128,1024]{2,1,0:T(8,128)(2,1)S(1)} %get-tuple-element.27), channel_id=1, source_target_pairs={{0,3},{1,0},{2,1},{3,2},{4,7},{5,4},{6,5},{7,6},{8,11},{9,8},{10,9... | collective-permute-start | bytes 1572872 | tf_op jit(solution)/shard_map/ppermute | solution.py:193
  72.1 21.4 %all-to-all-start.3 = ((bf16[8,128,128]{2,1,0:T(8,128)(2,1)}), bf16[8,128,128]{2,1,0:T(8,128)(2,1)S(1)}, u32[]{:S(2)}, u32[]{:S(2)}) async-start(bf16[8,128,128]{2,1,0:T(8,128)(2,1)} %shard_map.85), calls=%async_computation.3 | async-start | bytes 524288 | tf_op jit(solution)/shard_map/all_to_all | solution.py:335
  80.7 11.8 %copy-start = (s32[2048,4]{0,1:T(4,128)S(1)}, s32[2048,4]{0,1:T(4,128)}, u32[]{:S(2)}) copy-start(s32[2048,4]{0,1:T(4,128)} %param.11) | copy-start | bytes 98308
  80.7 11.8 %copy-start.1 = (f32[2048,4]{0,1:T(4,128)S(1)}, f32[2048,4]{0,1:T(4,128)}, u32[]{:S(2)}) copy-start(f32[2048,4]{0,1:T(4,128)} %param.12) | copy-start | bytes 98308
  82.0 11.7 %collective-permute-start.3 = (bf16[1,1024,128]{2,1,0:T(8,128)(2,1)S(1)}, bf16[1,1024,128]{2,1,0:T(8,128)(2,1)S(1)}, u32[]{:S(2)}, u32[]{:S(2)}) collective-permute-start(bf16[1,1024,128]{2,1,0:T(8,128)(2,1)S(1)} %get-tuple-element.30), channel_id=1, source_target_pairs={{0,1},{1,2},{2,3},{3,0},{4,5},{5,6},{6,7},{7,4},{8,9},{9,10},{10,1... | collective-permute-start | bytes 786440 | tf_op jit(solution)/shard_map/ppermute | solution.py:193
  85.2 12.1 %collective-permute-start.4 = (bf16[1,1024,128]{2,1,0:T(8,128)(2,1)S(1)}, bf16[1,1024,128]{2,1,0:T(8,128)(2,1)S(1)}, u32[]{:S(2)}, u32[]{:S(2)}) collective-permute-start(bf16[1,1024,128]{2,1,0:T(8,128)(2,1)S(1)} %get-tuple-element.31), channel_id=1, source_target_pairs={{0,2},{1,3},{2,0},{3,1},{4,6},{5,7},{6,4},{7,5},{8,10},{9,11},{10,... | collective-permute-start | bytes 786440 | tf_op jit(solution)/shard_map/ppermute | solution.py:193
  88.3 11.8 %collective-permute-start.5 = (bf16[1,1024,128]{2,1,0:T(8,128)(2,1)S(1)}, bf16[1,1024,128]{2,1,0:T(8,128)(2,1)S(1)}, u32[]{:S(2)}, u32[]{:S(2)}) collective-permute-start(bf16[1,1024,128]{2,1,0:T(8,128)(2,1)S(1)} %get-tuple-element.32), channel_id=1, source_target_pairs={{0,3},{1,0},{2,1},{3,2},{4,7},{5,4},{6,5},{7,6},{8,11},{9,8},{10,9... | collective-permute-start | bytes 786440 | tf_op jit(solution)/shard_map/ppermute | solution.py:193
  92.5 0.7 copy-start.2

commit v3 on v2

--- a/solution.py
+++ b/solution.py
@@ -12,8 +12,9 @@
 CAP = 4
 GROUP = 8
 PARAMS = pltpu.CompilerParams(vmem_limit_bytes=16 * 1024 * 1024)
-FIRST = {"z": lambda n: 13, "c": lambda n: n - 1, "y": lambda n: n // 2, "x": lambda n: n // 2}
+FIRST = {"z": lambda n: 15, "c": lambda n: n - 1, "y": lambda n: n // 2, "x": lambda n: n // 2}
 STEP = {"z": 1, "c": 1, "y": 1, "x": 1}
+BACK = 8
 REDUCE = [4, 7, 2, 5, 0, 3, 6, 1]
 GATHER = [4, 7, 2, 5, 0, 3, 6, 1]
 VMEM = pl.BlockSpec(memory_space=pltpu.VMEM)
@@ -58,6 +59,11 @@
         out_specs=VMEM if single else [VMEM] * len(outs),
         compiler_params=PARAMS,
     )(*args)
+
+
+def turned(rows, chips, first):
+    at = (first - FIRST["z"](chips)) % chips * (rows.shape[0] // chips)
+    return jnp.concatenate([rows[at:], rows[:at]], axis=0) if at else rows
 
 
 def place_of(index, axis):
@@ -85,33 +91,54 @@
     ]
 
 
-def deal(arrays, shifts, kernel=None, extra=(), extra_outs=()):
+def deal(arrays, shifts, kernels=(), extra=(), extra_outs=(), out=()):
     one = shape((len(arrays), *arrays[0].shape[1:]), BF)
     n, m, k = len(arrays), len(shifts), len(extra)
+    through = [shifts.index(d) for d in out] + ([m] if out else [])
+    shapes = [one] * m + list(extra_outs)
 
     def body(*refs):
         sources, small, rest = refs[:n], refs[n : n + k], refs[n + k :]
-        outs, held, sems, small_sems = rest[: len(rest) - k - 2], rest[-k - 2 : -2], *rest[-2:]
+        outs, rest = list(rest[: len(shapes)]), rest[len(shapes) :]
+        held, kept, (sems, small_sems, out_sems) = rest[:k], rest[k:-3], rest[-3:]
+        stores = []
+        for i, at in enumerate(through):
+            stores.append(pltpu.make_async_copy(kept[i], outs[at], out_sems.at[i]))
+            outs[at] = kept[i]
         fetches = [
             pltpu.make_async_copy(small[i], held[i], small_sems.at[i]) for i in range(k)
         ]
         copies = slice_copies(sources, outs[:m], shifts, sems)
-        for copy in fetches + copies:
+        ahead = sorted(range(m * n), key=lambda i: i // n not in through)
+        for copy in fetches + [copies[i] for i in ahead]:
             copy.start()
         for copy in fetches:
             copy.wait()
-        if kernel is not None:
-            kernel(*held, *outs[m:])
-        for copy in copies:
-            copy.wait()
+        for i, step in enumerate(kernels):
+            step(*held, *outs[m:])
+            if i == 0:
+                for store, at in reversed(list(zip(stores, through))):
+                    for copy in copies[at * n : (at + 1) * n]:
+                        copy.wait()
+                    store.start()
+        for i, copy in enumerate(copies):
+            if i // n not in through:
+                copy.wait()
+        for store in stores:
+            store.wait()
 
     return pl.pallas_call(
         body,
-        out_shape=[one] * m + list(extra_outs),
+        out_shape=shapes,
         in_specs=[HBM] * (n + k),
-        out_specs=[VMEM] * (m + len(extra_outs)),
+        out_specs=[HBM if i in through else VMEM for i in range(len(shapes))],
         scratch_shapes=[pltpu.VMEM(a.shape, a.dtype) for a in extra]
-        + [pltpu.SemaphoreType.DMA((m * n,)), pltpu.SemaphoreType.DMA((max(k, 1),))],
+        + [pltpu.VMEM(shapes[i].shape, BF) for i in through]
+        + [
+            pltpu.SemaphoreType.DMA((m * n,)),
+            pltpu.SemaphoreType.DMA((max(k, 1),)),
+            pltpu.SemaphoreType.DMA((max(len(through), 1),)),
+        ],
         compiler_params=PARAMS,
     )(*[in_hbm(a) for a in (*arrays, *extra)])
 
@@ -172,7 +199,8 @@
     last_ref[...] = jnp.broadcast_to(gain_ref[...], last_ref.shape)
 
 
-def three_rows(gain, tail_ref):
+def tail_kernel(gain_ref, tail_ref):
+    gain = gain_ref[...]
     high = gain.astype(BF).astype(F32)
     middle = (gain - high).astype(BF).astype(F32)
     low = gain - high - middle
@@ -181,11 +209,12 @@
     tail_ref[...] = tail.astype(BF)
 
 
-def routing_kernel(routes_ref, tok_ref, gain_ref, out_ref, place_ref, sel_ref, tail_ref):
-    ids = [routes_ref[:, k, :] for k in range(CAP)]
-    dispatch(ids, tok_ref, out_ref, place_ref)
-    select_table(ids, sel_ref)
-    three_rows(gain_ref[...], tail_ref)
+def dispatch_step(routes_ref, tok_ref, out_ref, place_ref, sel_ref):
+    dispatch([routes_ref[:, k, :] for k in range(CAP)], tok_ref, out_ref, place_ref)
+
+
+def select_step(routes_ref, tok_ref, out_ref, place_ref, sel_ref):
+    select_table([routes_ref[:, k, :] for k in range(CAP)], sel_ref)
 
 
 def passed(piece, d, axis):
@@ -301,11 +330,13 @@
             [parts_ref[e, q * 16 : (q + 1) * 16, :] for e in range(GROUP)], axis=0
         )
         total = total + dot_rows(sel_ref[q], rows)
-    out_ref[...] = total.astype(BF)
+    out_ref[...] = turned(total, lax.axis_size("z"), BACK).astype(BF)
 
 
 def place_kernel(ret_ref, place_ref, comb_ref, squares_ref):
-    full = dot_rows(place_ref[...], ret_ref[...])
+    chips = lax.axis_size("z")
+    back = turned(ret_ref[...], chips, 2 * FIRST["z"](chips) - BACK)
+    full = dot_rows(place_ref[...], back)
     comb_ref[...] = full[0:HALF] + full[HALF:LANES]
     squares = jnp.sum(full * full, axis=1, keepdims=True)
     flat = jnp.transpose(jnp.broadcast_to(squares, (LANES, LANES)))[0:1, :]
@@ -344,21 +375,22 @@
     weights = jnp.transpose(route_weights.reshape(chips, LANES, CAP), (0, 2, 1))
 
     square = shape((LANES, LANES), BF)
-    own, near, far, back, outgoing, place, sel, tail = deal(
+    own, near, far, back, outgoing, place, sel = deal(
         [w_gate, w_up],
         [0, 1, 2, 3],
-        routing_kernel,
-        (routes, tokens, in_gain.reshape(1, local)),
+        (dispatch_step, select_step),
+        (routes, tokens),
         (
             square,
             square,
             shape((CAP, LANES, LANES), BF),
-            shape((8, LANES), BF),
         ),
+        out=(1,),
     )
     gate_up = [own, passed(near, 1, "x"), passed(far, 2, "x"), passed(back, 3, "x")]
     own, near, far, back = deal([w_down], [0, 1, 2, 3])
     down = [own, passed(near, 1, "x"), passed(far, 2, "x"), passed(back, 3, "x")]
+    tail = call(tail_kernel, shape((8, LANES), BF), in_gain.reshape(1, local))
     arrived = exchange(outgoing.reshape(chips, GROUP, local), ("z",))
     slots = call(
         select_kernel, shape((GROUP, 72, LANES), BF), arrived.reshape(LANES, local), sel, tail
@@ -387,7 +419,8 @@
     answers = call(down_kernel, shape((GROUP, 64, LANES), BF), act, scale, own, *others)
     answers = exchange(answers, ("c", "x"))
     mixed = call(combine_kernel, shape((LANES, local), BF), answers, sel)
-    returned = exchange(mixed.reshape(chips, GROUP, local), ("z",))
+    order = [(BACK + i) % chips for i in range(chips)]
+    returned = exchange(mixed.reshape(chips, GROUP, local), ("z",), order)
     combined, squares = call(
         place_kernel,
         [shape((HALF, local), F32), shape((ys * xs, 1, LANES), F32)],

time: 137 us -> 139 us (1.015)
  blocking collectives: 82.1 us -> 63.9 us
  waiting for transfers between devices: 6.35 us -> 15.7 us
  starting transfers between devices: 40.1 us -> 49.3 us
    all_to_all x6 -> x5, blocking collectives: 82.1 us -> 63.9 us  [exchange(): lax.all_to_all(value, axes, 0, 0, tiled=True, axis_index_groups=groups)]
    all_to_all x1 -> x2, waiting for transfers between devices: 0.01 us -> 9.31 us  [exchange(): lax.all_to_all(value, axes, 0, 0, tiled=True, axis_index_groups=groups)]
    all_to_all x1 -> x2, starting transfers between devices: 8.67 us -> 17.8 us  [exchange(): lax.all_to_all(value, axes, 0, 0, tiled=True, axis_index_groups=groups)]
    pallas_call x9 -> x10, Pallas kernels: 3.92 us -> 3.91 us  [call(): pl.pallas_call(kernel, out_shape=outs, in_specs=[VMEM] * len(args), out_s...]
  transfers between devices with their start and end apart: 7 -> 8, of which waited for: 2 -> 3; matrix products, arithmetic and copies ran while one was open for 0% -> 0% of each run, Pallas kernels for 1% -> 1%
where the time goes in v3:
time: 139 us
  blocking collectives  63.9 us (46%)
  starting transfers between devices  49.3 us (35%)
  waiting for transfers between devices  15.7 us (11%)
  Pallas kernels  8.44 us (6%)
    all_to_all x5, blocking collectives, exchange(): lax.all_to_all(value, axes, 0, 0, tiled=True, axis_index_groups=groups)  63.9 us
    ppermute x6, starting transfers between devices, passed(): return lax.ppermute(piece, axis, [(i, (i + d) % n) for i in range(n)])  31.5 us
    all_to_all x2, starting transfers between devices, exchange(): lax.all_to_all(value, axes, 0, 0, tiled=True, axis_index_groups=groups)  17.8 us
    all_to_all x2, waiting for transfers between devices, exchange(): lax.all_to_all(value, axes, 0, 0, tiled=True, axis_index_groups=groups)  9.31 us
    ppermute x6, waiting for transfers between devices, passed(): return lax.ppermute(piece, axis, [(i, (i + d) % n) for i in range(n)])  6.35 us
    pallas_call x2, Pallas kernels, deal(): pl.pallas_call(body, out_shape=shapes, in_specs=[HBM] * (n + k), out_spec...  4.52 us
    pallas_call x10, Pallas kernels, call(): pl.pallas_call(kernel, out_shape=outs, in_specs=[VMEM] * len(args), out_s...  3.91 us
  transfers between devices with their start and end apart: 8, of which 3 were waited for; matrix products, arithmetic and copies ran while one was open for 0% of the time, Pallas kernels for 1%

profile of v3, /device:TPU:2, one launch (start us, length us, event | category | flops | bytes accessed | tf_op | source)
XLA Modules:
  0.0 138.8 jit_solution(2064248462895249246)
XLA Ops:
  0.0 3.3 %shard_map.82 = (bf16[2,128,1024]{2,1,0:T(8,128)(2,1)S(1)}, bf16[2,128,1024]{2,1,0:T(8,128)(2,1)}, bf16[2,128,1024]{2,1,0:T(8,128)(2,1)}, bf16[2,128,1024]{2,1,0...) custom-call(bf16[4,128,1024]{2,1,0:T(8,128)(2,1)} %refs_0_.2, ...), custom_call_target="tpu_custom_call" | custom-call | tf_op jit(solution)/shard_map/pallas_call | solution.py:130
  3.3 3.4 %collective-permute-start = (bf16[2,128,1024]{2,1,0:T(8,128)(2,1)}, bf16[2,128,1024]{2,1,0:T(8,128)(2,1)S(1)}, u32[]{:S(2)}, u32[]{:S(2)}) collective-permute-start(bf16[2,128,1024]{2,1,0:T(8,128)(2,1)} %get-tuple-element.23), channel_id=1, source_target_pairs={{0,1},{1,2},{2,3},{3,0},{4,5},{5,6},{6,7},{7,4},{8,9},{9,10},{10,1... | collective-permute-start | bytes 1572872 | tf_op jit(solution)/shard_map/ppermute | solution.py:222
  6.7 15.6 %collective-permute-start.1 = (bf16[2,128,1024]{2,1,0:T(8,128)(2,1)}, bf16[2,128,1024]{2,1,0:T(8,128)(2,1)S(1)}, u32[]{:S(2)}, u32[]{:S(2)}) collective-permute-start(bf16[2,128,1024]{2,1,0:T(8,128)(2,1)} %get-tuple-element.24), channel_id=1, source_target_pairs={{0,2},{1,3},{2,0},{3,1},{4,6},{5,7},{6,4},{7,5},{8,10},{9,11},{10,... | collective-permute-start | bytes 1572872 | tf_op jit(solution)/shard_map/ppermute | solution.py:222
  22.4 1.9 %collective-permute-start.2 = (bf16[2,128,1024]{2,1,0:T(8,128)(2,1)S(1)}, bf16[2,128,1024]{2,1,0:T(8,128)(2,1)S(1)}, u32[]{:S(2)}, u32[]{:S(2)}) collective-permute-start(bf16[2,128,1024]{2,1,0:T(8,128)(2,1)S(1)} %get-tuple-element.25), channel_id=1, source_target_pairs={{0,3},{1,0},{2,1},{3,2},{4,7},{5,4},{6,5},{7,6},{8,11},{9,8},{10,9... | collective-permute-start | bytes 1572872 | tf_op jit(solution)/shard_map/ppermute | solution.py:222
  24.3 9.1 %all-to-all-start = ((bf16[16,8,128]{2,1,0:T(8,128)(2,1)}), bf16[16,8,128]{2,1,0:T(8,128)(2,1)S(1)}, u32[]{:S(2)}, u32[]{:S(2)}) async-start(bf16[16,8,128]{2,1,0:T(8,128)(2,1)} %bitcast.2), calls=%async_computation | async-start | bytes 65536 | tf_op jit(solution)/shard_map/all_to_all | solution.py:366
  33.4 0.0 copy-start.3
  33.4 0.6 copy-done.3
  34.1 9.3 %all-to-all-done = bf16[16,8,128]{2,1,0:T(8,128)(2,1)S(1)} async-done(((bf16[16,8,128]{2,1,0:T(8,128)(2,1)}), bf16[16,8,128]{2,1,0:T(8,128)(2,1)S(1)}, u32[]{:S(2)}, u32[]{:S(2)}) %all-to-all-start) | async-done | bytes 32800 | tf_op jit(solution)/shard_map/all_to_all | solution.py:366
  43.4 0.2 shard_map.84
  43.6 8.5 %all_to_all.35.rows_ref = bf16[8,72,128]{2,1,0:T(8,128)(2,1)S(1)} all-to-all(bf16[8,72,128]{2,1,0:T(8,128)(2,1)S(1)} %shard_map.84), channel_id=1, replica_groups={{34,35,32,33,2,3,0,1},{38,39,36,37,6,7,4,5},{42,43,40,41,10,11,8,9},{46..., dimensions={0} | all-to-all | bytes 294912 | tf_op jit(solution)/shard_map/all_to_all | solution.py:366
  52.1 0.0 collective-permute-done.refs_1_
  52.1 0.0 collective-permute-done.1.refs_2_
  52.1 0.0 collective-permute-done.2.refs_3_
  52.1 0.7 shard_map.85
  52.8 20.8 %all_to_all.36.refs_0_ = bf16[8,264,128]{2,1,0:T(8,128)(2,1)S(1)} all-to-all(bf16[8,264,128]{2,1,0:T(8,128)(2,1)S(1)} %shard_map.85), channel_id=1, replica_groups={{16,28,8,20,0,12,24,4},{17,29,9,21,1,13,25,5},{18,30,10,22,2,14,26,6},{..., dimensions={0} | all-to-all | bytes 1081344 | tf_op jit(solution)/shard_map/all_to_all | solution.py:366
  73.5 0.9 shard_map.86
  74.5 8.7 %all-to-all-start.3 = ((bf16[8,128,128]{2,1,0:T(8,128)(2,1)}), bf16[8,128,128]{2,1,0:T(8,128)(2,1)S(1)}, u32[]{:S(2)}, u32[]{:S(2)}) async-start(bf16[8,128,128]{2,1,0:T(8,128)(2,1)} %shard_map.86), calls=%async_computation.3 | async-start | bytes 524288 | tf_op jit(solution)/shard_map/all_to_all | solution.py:366
  83.2 0.0 copy-start
  83.2 0.0 copy-start.1
  83.2 1.2 shard_map.88
  84.4 3.3 %collective-permute-start.3 = (bf16[1,1024,128]{2,1,0:T(8,128)(2,1)S(1)}, bf16[1,1024,128]{2,1,0:T(8,128)(2,1)S(1)}, u32[]{:S(2)}, u32[]{:S(2)}) collective-permute-start(bf16[1,1024,128]{2,1,0:T(8,128)(2,1)S(1)} %get-tuple-element.28), channel_id=1, source_target_pairs={{0,1},{1,2},{2,3},{3,0},{4,5},{5,6},{6,7},{7,4},{8,9},{9,10},{10,1... | collective-permute-start | bytes 786440 | tf_op jit(solution)/shard_map/ppermute | solution.py:222
  87.7 3.0 %collective-permute-start.4 = (bf16[1,1024,128]{2,1,0:T(8,128)(2,1)S(1)}, bf16[1,1024,128]{2,1,0:T(8,128)(2,1)S(1)}, u32[]{:S(2)}, u32[]{:S(2)}) collective-permute-start(bf16[1,1024,128]{2,1,0:T(8,128)(2,1)S(1)} %get-tuple-element.29), channel_id=1, source_target_pairs={{0,2},{1,3},{2,0},{3,1},{4,6},{5,7},{6,4},{7,5},{8,10},{9,11},{10,... | collective-permute-start | bytes 786440 | tf_op jit(solution)/shard_map/ppermute | solution.py:222
  90.7 4.3 %collective-permute-start.5 = (bf16[1,1024,128]{2,1,0:T(8,128)(2,1)S(1)}, bf16[1,1024,128]{2,1,0:T(8,128)(2,1)S(1)}, u32[]{:S(2)}, u32[]{:S(2)}) collective-permute-start(bf16[1,1024,128]{2,1,0:T(8,128)(2,1)S(1)} %get-tuple-element.30), channel_id=1, source_target_pairs={{0,3},{1,0},{2,1},{3,2},{4,7},{5,4},{6,5},{7,6},{8,11},{9,8},{10,9... | collective-permute-start | bytes 786440 | tf_op jit(solution)/shard_map/ppermute | solution.py:222
  95.0 0.0 copy-start.2
  95.0 0.0 copy-done
  95.0 0.0 copy-done.1
  95.0 0.6 copy-done.2
  95.6 0.2 shard_map.87
  95.9 0.0 all-to-all-done.3.act_ref
  95.9 0.2 shard_map.89.own_ref
  96.1 0.0 collective-permute-done.3.refs_0_
  96.1 3.6 %collective-permute-done.4.refs_1_ = bf16[1,1024,128]{2,1,0:T(8,128)(2,1)S(1)} collective-permute-done((bf16[1,1024,128]{2,1,0:T(8,128)(2,1)S(1)}, bf16[1,1024,128]{2,1,0:T(8,128)(2,1)S(1)}, u32[]{:S(2)}, u32[]{:S(2)}) %collective-permute-start.4) | collective-permute-done | bytes 262176 | tf_op jit(solution)/shard_map/ppermute | solution.py:222
  99.8 2.7 %collective-permute-done.5.refs_2_ = bf16[1,1024,128]{2,1,0:T(8,128)(2,1)S(1)} collective-permute-done((bf16[1,1024,128]{2,1,0:T(8,128)(2,1)S(1)}, bf16[1,1024,128]{2,1,0:T(8,128)(2,1)S(1)}, u32[]{:S(2)}, u32[]{:S(2)}) %collective-permute-start.5) | collective-permute-done | bytes 262176 | tf_op jit(solution)/shard_map/ppermute | solution.py:222
  102.5 0.4 shard_map.90
  102.8 7.7 %all_to_all.37.parts_ref = bf16[8,64,128]{2,1,0:T(8,128)(2,1)S(1)} all-to-all(bf16[8,64,128]{2,1,0:T(8,128)(2,1)S(1)} %shard_map.90), channel_id=1, replica_groups={{34,35,32,33,2,3,0,1},{38,39,36,37,6,7,4,5},{42,43,40,41,10,11,8,9},{46..., dimensions={0} | all-to-all | bytes 262144 | tf_op jit(solution)/shard_map/all_to_all | solution.py:366
  110.5 0.2 shard_map.91
  110.8 14.8 %all_to_all.38 = bf16[16,8,128]{2,1,0:T(8,128)(2,1)S(1)} all-to-all(bf16[16,8,128]{2,1,0:T(8,128)(2,1)S(1)} %bitcast.15), channel_id=1, replica_groups={{512,576,640,704,768,832,896,960,0,64,128,192,256,320,384,448},{513,577..., dimensions={0} | all-to-all | bytes 65536 | tf_op jit(solution)/shard_map/all_to_all | solution.py:366
  125.6 0.3 shard_map.92
  125.9 12.1 %all_to_all.39.refs_0_ = f32[32,1,128]{2,1,0:T(1,128)S(1)} all-to-all(f32[32,1,128]{2,1,0:T(1,128)S(1)} %get-tuple-element.32), channel_id=1, replica_groups={{18,19,16,17,22,23,20,21,26,27,24,25,30,31,28,29,2,3,0,1,6,7,4,5,10,11,..., dimensions={0} | all-to-all | bytes 32768 | tf_op jit(solution)/shard_map/all_to_all | solution.py:366
  138.0 0.8 shard_map.93
  (1 shorter events, 0.0 us)
Async XLA Ops:
  3.3 48.8 %collective-permute-start = (bf16[2,128,1024]{2,1,0:T(8,128)(2,1)}, bf16[2,128,1024]{2,1,0:T(8,128)(2,1)S(1)}, u32[]{:S(2)}, u32[]{:S(2)}) collective-permute-start(bf16[2,128,1024]{2,1,0:T(8,128)(2,1)} %get-tuple-element.23), channel_id=1, source_target_pairs={{0,1},{1,2},{2,3},{3,0},{4,5},{5,6},{6,7},{7,4},{8,9},{9,10},{10,1... | collective-permute-start | bytes 1572872 | tf_op jit(solution)/shard_map/ppermute | solution.py:222
  6.7 45.4 %collective-permute-start.1 = (bf16[2,128,1024]{2,1,0:T(8,128)(2,1)}, bf16[2,128,1024]{2,1,0:T(8,128)(2,1)S(1)}, u32[]{:S(2)}, u32[]{:S(2)}) collective-permute-start(bf16[2,128,1024]{2,1,0:T(8,128)(2,1)} %get-tuple-element.24), channel_id=1, source_target_pairs={{0,2},{1,3},{2,0},{3,1},{4,6},{5,7},{6,4},{7,5},{8,10},{9,11},{10,... | collective-permute-start | bytes 1572872 | tf_op jit(solution)/shard_map/ppermute | solution.py:222
  22.4 29.7 %collective-permute-start.2 = (bf16[2,128,1024]{2,1,0:T(8,128)(2,1)S(1)}, bf16[2,128,1024]{2,1,0:T(8,128)(2,1)S(1)}, u32[]{:S(2)}, u32[]{:S(2)}) collective-permute-start(bf16[2,128,1024]{2,1,0:T(8,128)(2,1)S(1)} %get-tuple-element.25), channel_id=1, source_target_pairs={{0,3},{1,0},{2,1},{3,2},{4,7},{5,4},{6,5},{7,6},{8,11},{9,8},{10,9... | collective-permute-start | bytes 1572872 | tf_op jit(solution)/shard_map/ppermute | solution.py:222
  24.3 19.1 %all-to-all-start = ((bf16[16,8,128]{2,1,0:T(8,128)(2,1)}), bf16[16,8,128]{2,1,0:T(8,128)(2,1)S(1)}, u32[]{:S(2)}, u32[]{:S(2)}) async-start(bf16[16,8,128]{2,1,0:T(8,128)(2,1)} %bitcast.2), calls=%async_computation | async-start | bytes 65536 | tf_op jit(solution)/shard_map/all_to_all | solution.py:366
  33.4 0.7 copy-start.3
  74.5 21.4 %all-to-all-start.3 = ((bf16[8,128,128]{2,1,0:T(8,128)(2,1)}), bf16[8,128,128]{2,1,0:T(8,128)(2,1)S(1)}, u32[]{:S(2)}, u32[]{:S(2)}) async-start(bf16[8,128,128]{2,1,0:T(8,128)(2,1)} %shard_map.86), calls=%async_computation.3 | async-start | bytes 524288 | tf_op jit(solution)/shard_map/all_to_all | solution.py:366
  83.2 11.8 %copy-start = (s32[2048,4]{0,1:T(4,128)S(1)}, s32[2048,4]{0,1:T(4,128)}, u32[]{:S(2)}) copy-start(s32[2048,4]{0,1:T(4,128)} %param.11) | copy-start | bytes 98308
  83.2 11.8 %copy-start.1 = (f32[2048,4]{0,1:T(4,128)S(1)}, f32[2048,4]{0,1:T(4,128)}, u32[]{:S(2)}) copy-start(f32[2048,4]{0,1:T(4,128)} %param.12) | copy-start | bytes 98308
  84.4 11.7 %collective-permute-start.3 = (bf16[1,1024,128]{2,1,0:T(8,128)(2,1)S(1)}, bf16[1,1024,128]{2,1,0:T(8,128)(2,1)S(1)}, u32[]{:S(2)}, u32[]{:S(2)}) collective-permute-start(bf16[1,1024,128]{2,1,0:T(8,128)(2,1)S(1)} %get-tuple-element.28), channel_id=1, source_target_pairs={{0,1},{1,2},{2,3},{3,0},{4,5},{5,6},{6,7},{7,4},{8,9},{9,10},{10,1... | collective-permute-start | bytes 786440 | tf_op jit(solution)/shard_map/ppermute | solution.py:222
  87.7 12.1 %collective-permute-start.4 = (bf16[1,1024,128]{2,1,0:T(8,128)(2,1)S(1)}, bf16[1,1024,128]{2,1,0:T(8,128)(2,1)S(1)}, u32[]{:S(2)}, u32[]{:S(2)}) collective-permute-start(bf16[1,1024,128]{2,1,0:T(8,128)(2,1)S(1)} %get-tuple-element.29), channel_id=1, source_target_pairs={{0,2},{1,3},{2,0},{3,1},{4,6},{5,7},{6,4},{7,5},{8,10},{9,11},{10,... | collective-permute-start | bytes 786440 | tf_op jit(solution)/shard_map/ppermute | solution.py:222
  90.7 11.8 %collective-permute-start.5 = (bf16[1,1024,128]{2,1,0:T(8,128)(2,1)S(1)}, bf16[1,1024,128]{2,1,0:T(8,128)(2,1)S(1)}, u32[]{:S(2)}, u32[]{:S(2)}) collective-permute-start(bf16[1,1024,128]{2,1,0:T(8,128)(2,1)S(1)} %get-tuple-element.30), channel_id=1, source_target_pairs={{0,3},{1,0},{2,1},{3,2},{4,7},{5,4},{6,5},{7,6},{8,11},{9,8},{10,9... | collective-permute-start | bytes 786440 | tf_op jit(solution)/shard_map/ppermute | solution.py:222
  95.0 0.7 copy-start.2

commit v4 on v3

--- a/solution.py
+++ b/solution.py
@@ -209,12 +209,13 @@
     tail_ref[...] = tail.astype(BF)
 
 
-def dispatch_step(routes_ref, tok_ref, out_ref, place_ref, sel_ref):
+def dispatch_step(routes_ref, tok_ref, out_ref, place_ref):
     dispatch([routes_ref[:, k, :] for k in range(CAP)], tok_ref, out_ref, place_ref)
 
 
-def select_step(routes_ref, tok_ref, out_ref, place_ref, sel_ref):
+def select_step(routes_ref, gain_ref, sel_ref, tail_ref):
     select_table([routes_ref[:, k, :] for k in range(CAP)], sel_ref)
+    tail_kernel(gain_ref, tail_ref)
 
 
 def passed(piece, d, axis):
@@ -375,22 +376,19 @@
     weights = jnp.transpose(route_weights.reshape(chips, LANES, CAP), (0, 2, 1))
 
     square = shape((LANES, LANES), BF)
-    own, near, far, back, outgoing, place, sel = deal(
+    near, far, back, outgoing, place = deal(
+        [w_gate, w_up], [1, 2, 3], (dispatch_step,), (routes, tokens), (square, square), out=(1,)
+    )
+    own, sel, tail = deal(
         [w_gate, w_up],
-        [0, 1, 2, 3],
-        (dispatch_step, select_step),
-        (routes, tokens),
-        (
-            square,
-            square,
-            shape((CAP, LANES, LANES), BF),
-        ),
-        out=(1,),
+        [0],
+        (select_step,),
+        (routes, in_gain.reshape(1, local)),
+        (shape((CAP, LANES, LANES), BF), shape((8, LANES), BF)),
     )
     gate_up = [own, passed(near, 1, "x"), passed(far, 2, "x"), passed(back, 3, "x")]
     own, near, far, back = deal([w_down], [0, 1, 2, 3])
     down = [own, passed(near, 1, "x"), passed(far, 2, "x"), passed(back, 3, "x")]
-    tail = call(tail_kernel, shape((8, LANES), BF), in_gain.reshape(1, local))
     arrived = exchange(outgoing.reshape(chips, GROUP, local), ("z",))
     slots = call(
         select_kernel, shape((GROUP, 72, LANES), BF), arrived.reshape(LANES, local), sel, tail

time: 139 us -> 139 us (level)
    pallas_call x2 -> x3, Pallas kernels: 4.52 us -> 5.8 us  [deal(): pl.pallas_call(body, out_shape=shapes, in_specs=[HBM] * (n + k), out_spec...]
    pallas_call x10 -> x9, Pallas kernels: 3.91 us -> 3.9 us  [call(): pl.pallas_call(kernel, out_shape=outs, in_specs=[VMEM] * len(args), out_s...]
  transfers between devices with their start and end apart: 8 -> 8, of which waited for: 3 -> 3; matrix products, arithmetic and copies ran while one was open for 0% -> 0% of each run, Pallas kernels for 1% -> 2%
where the time goes in v4:
time: 139 us
  blocking collectives  63.9 us (46%)
  starting transfers between devices  49.3 us (35%)
  waiting for transfers between devices  14.9 us (11%)
  Pallas kernels  9.7 us (7%)
    all_to_all x5, blocking collectives, exchange(): lax.all_to_all(value, axes, 0, 0, tiled=True, axis_index_groups=groups)  63.9 us
    ppermute x6, starting transfers between devices, passed(): return lax.ppermute(piece, axis, [(i, (i + d) % n) for i in range(n)])  31.5 us
    all_to_all x2, starting transfers between devices, exchange(): lax.all_to_all(value, axes, 0, 0, tiled=True, axis_index_groups=groups)  17.9 us
    all_to_all x2, waiting for transfers between devices, exchange(): lax.all_to_all(value, axes, 0, 0, tiled=True, axis_index_groups=groups)  8.53 us
    ppermute x6, waiting for transfers between devices, passed(): return lax.ppermute(piece, axis, [(i, (i + d) % n) for i in range(n)])  6.35 us
    pallas_call x3, Pallas kernels, deal(): pl.pallas_call(body, out_shape=shapes, in_specs=[HBM] * (n + k), out_spec...  5.8 us
    pallas_call x9, Pallas kernels, call(): pl.pallas_call(kernel, out_shape=outs, in_specs=[VMEM] * len(args), out_s...  3.9 us
  transfers between devices with their start and end apart: 8, of which 3 were waited for; matrix products, arithmetic and copies ran while one was open for 0% of the time, Pallas kernels for 2%

profile of v4, /device:TPU:2, one launch (start us, length us, event | category | flops | bytes accessed | tf_op | source)
XLA Modules:
  0.0 138.6 jit_solution(5690896928039425399)
XLA Ops:
  0.0 3.1 %shard_map.82 = (bf16[2,128,1024]{2,1,0:T(8,128)(2,1)}, bf16[2,128,1024]{2,1,0:T(8,128)(2,1)}, bf16[2,128,1024]{2,1,0:T(8,128)(2,1)S(1)}, bf16[128,128]{1,0:T(8,128)(2,1)}, bf16[128,128]{1,0:T(8,128)(2,1)S(1)}) custom-call(bf16[4,128,1024]{2,1,0:T(8,128)(2,1)} %refs_0_.4, bf16[4,128,1024]{2,1,0:T(8,128)(2,1)} %refs_1_.3, s32[16,4,128]{2,1,0:T(4,128)} %bitcast.12, ...), custom_call_target="tpu_custom_call" | custom-call | tf_op jit(solution)/shard_map/pallas_call | solution.py:130
  3.1 3.4 %collective-permute-start = (bf16[2,128,1024]{2,1,0:T(8,128)(2,1)}, bf16[2,128,1024]{2,1,0:T(8,128)(2,1)S(1)}, u32[]{:S(2)}, u32[]{:S(2)}) collective-permute-start(bf16[2,128,1024]{2,1,0:T(8,128)(2,1)} %get-tuple-element.25), channel_id=1, source_target_pairs={{0,1},{1,2},{2,3},{3,0},{4,5},{5,6},{6,7},{7,4},{8,9},{9,10},{10,1... | collective-permute-start | bytes 1572872 | tf_op jit(solution)/shard_map/ppermute | solution.py:223
  6.6 15.6 %collective-permute-start.1 = (bf16[2,128,1024]{2,1,0:T(8,128)(2,1)}, bf16[2,128,1024]{2,1,0:T(8,128)(2,1)S(1)}, u32[]{:S(2)}, u32[]{:S(2)}) collective-permute-start(bf16[2,128,1024]{2,1,0:T(8,128)(2,1)} %get-tuple-element.26), channel_id=1, source_target_pairs={{0,2},{1,3},{2,0},{3,1},{4,6},{5,7},{6,4},{7,5},{8,10},{9,11},{10,... | collective-permute-start | bytes 1572872 | tf_op jit(solution)/shard_map/ppermute | solution.py:223
  22.2 1.9 %collective-permute-start.2 = (bf16[2,128,1024]{2,1,0:T(8,128)(2,1)S(1)}, bf16[2,128,1024]{2,1,0:T(8,128)(2,1)S(1)}, u32[]{:S(2)}, u32[]{:S(2)}) collective-permute-start(bf16[2,128,1024]{2,1,0:T(8,128)(2,1)S(1)} %get-tuple-element.27), channel_id=1, source_target_pairs={{0,3},{1,0},{2,1},{3,2},{4,7},{5,4},{6,5},{7,6},{8,11},{9,8},{10,9... | collective-permute-start | bytes 1572872 | tf_op jit(solution)/shard_map/ppermute | solution.py:223
  24.1 9.2 %all-to-all-start = ((bf16[16,8,128]{2,1,0:T(8,128)(2,1)}), bf16[16,8,128]{2,1,0:T(8,128)(2,1)S(1)}, u32[]{:S(2)}, u32[]{:S(2)}) async-start(bf16[16,8,128]{2,1,0:T(8,128)(2,1)} %bitcast.2), calls=%async_computation | async-start | bytes 65536 | tf_op jit(solution)/shard_map/all_to_all | solution.py:367
  33.3 1.4 %shard_map.83 = (bf16[2,128,1024]{2,1,0:T(8,128)(2,1)S(1)}, bf16[4,128,128]{2,1,0:T(8,128)(2,1)S(1)}, bf16[8,128]{1,0:T(8,128)(2,1)S(1)}) custom-call(bf16[4,128,1024]{2,1,0:T(8,128)(2,1)} %refs_0_.4, bf16[4,128,1024]{2,1,0:T(8,128)(2,1)} %refs_1_.3, s32[16,4,128]{2,1,0:T(4,128)} %bitcast.13, f32[1,128]{1,0:T(1,128)} %bitcast.20), custom_call_target="tpu_custom_call" | custom-call | tf_op jit(solution)/shard_map/pallas_call | solution.py:130
  34.7 8.5 %all-to-all-done = bf16[16,8,128]{2,1,0:T(8,128)(2,1)S(1)} async-done(((bf16[16,8,128]{2,1,0:T(8,128)(2,1)}), bf16[16,8,128]{2,1,0:T(8,128)(2,1)S(1)}, u32[]{:S(2)}, u32[]{:S(2)}) %all-to-all-start) | async-done | bytes 32800 | tf_op jit(solution)/shard_map/all_to_all | solution.py:367
  43.3 0.2 shard_map.84
  43.4 8.5 %all_to_all.35.rows_ref = bf16[8,72,128]{2,1,0:T(8,128)(2,1)S(1)} all-to-all(bf16[8,72,128]{2,1,0:T(8,128)(2,1)S(1)} %shard_map.84), channel_id=1, replica_groups={{34,35,32,33,2,3,0,1},{38,39,36,37,6,7,4,5},{42,43,40,41,10,11,8,9},{46..., dimensions={0} | all-to-all | bytes 294912 | tf_op jit(solution)/shard_map/all_to_all | solution.py:367
  51.9 0.0 collective-permute-done.refs_1_
  51.9 0.0 collective-permute-done.1.refs_2_
  51.9 0.0 collective-permute-done.2.refs_3_
  51.9 0.7 shard_map.85
  52.6 20.8 %all_to_all.36.refs_0_ = bf16[8,264,128]{2,1,0:T(8,128)(2,1)S(1)} all-to-all(bf16[8,264,128]{2,1,0:T(8,128)(2,1)S(1)} %shard_map.85), channel_id=1, replica_groups={{16,28,8,20,0,12,24,4},{17,29,9,21,1,13,25,5},{18,30,10,22,2,14,26,6},{..., dimensions={0} | all-to-all | bytes 1081344 | tf_op jit(solution)/shard_map/all_to_all | solution.py:367
  73.4 0.9 shard_map.86
  74.3 8.7 %all-to-all-start.3 = ((bf16[8,128,128]{2,1,0:T(8,128)(2,1)}), bf16[8,128,128]{2,1,0:T(8,128)(2,1)S(1)}, u32[]{:S(2)}, u32[]{:S(2)}) async-start(bf16[8,128,128]{2,1,0:T(8,128)(2,1)} %shard_map.86), calls=%async_computation.3 | async-start | bytes 524288 | tf_op jit(solution)/shard_map/all_to_all | solution.py:367
  83.0 0.0 copy-start
  83.0 0.0 copy-start.1
  83.0 1.2 shard_map.88
  84.3 3.3 %collective-permute-start.3 = (bf16[1,1024,128]{2,1,0:T(8,128)(2,1)S(1)}, bf16[1,1024,128]{2,1,0:T(8,128)(2,1)S(1)}, u32[]{:S(2)}, u32[]{:S(2)}) collective-permute-start(bf16[1,1024,128]{2,1,0:T(8,128)(2,1)S(1)} %get-tuple-element.30), channel_id=1, source_target_pairs={{0,1},{1,2},{2,3},{3,0},{4,5},{5,6},{6,7},{7,4},{8,9},{9,10},{10,1... | collective-permute-start | bytes 786440 | tf_op jit(solution)/shard_map/ppermute | solution.py:223
  87.5 3.0 %collective-permute-start.4 = (bf16[1,1024,128]{2,1,0:T(8,128)(2,1)S(1)}, bf16[1,1024,128]{2,1,0:T(8,128)(2,1)S(1)}, u32[]{:S(2)}, u32[]{:S(2)}) collective-permute-start(bf16[1,1024,128]{2,1,0:T(8,128)(2,1)S(1)} %get-tuple-element.31), channel_id=1, source_target_pairs={{0,2},{1,3},{2,0},{3,1},{4,6},{5,7},{6,4},{7,5},{8,10},{9,11},{10,... | collective-permute-start | bytes 786440 | tf_op jit(solution)/shard_map/ppermute | solution.py:223
  90.6 4.3 %collective-permute-start.5 = (bf16[1,1024,128]{2,1,0:T(8,128)(2,1)S(1)}, bf16[1,1024,128]{2,1,0:T(8,128)(2,1)S(1)}, u32[]{:S(2)}, u32[]{:S(2)}) collective-permute-start(bf16[1,1024,128]{2,1,0:T(8,128)(2,1)S(1)} %get-tuple-element.32), channel_id=1, source_target_pairs={{0,3},{1,0},{2,1},{3,2},{4,7},{5,4},{6,5},{7,6},{8,11},{9,8},{10,9... | collective-permute-start | bytes 786440 | tf_op jit(solution)/shard_map/ppermute | solution.py:223
  94.8 0.0 copy-start.2
  94.8 0.0 copy-done
  94.8 0.0 copy-done.1
  94.8 0.6 copy-done.2
  95.5 0.2 shard_map.87
  95.7 0.0 all-to-all-done.3.act_ref
  95.7 0.2 shard_map.89.own_ref
  96.0 0.0 collective-permute-done.3.refs_0_
  96.0 3.6 %collective-permute-done.4.refs_1_ = bf16[1,1024,128]{2,1,0:T(8,128)(2,1)S(1)} collective-permute-done((bf16[1,1024,128]{2,1,0:T(8,128)(2,1)S(1)}, bf16[1,1024,128]{2,1,0:T(8,128)(2,1)S(1)}, u32[]{:S(2)}, u32[]{:S(2)}) %collective-permute-start.4) | collective-permute-done | bytes 262176 | tf_op jit(solution)/shard_map/ppermute | solution.py:223
  99.6 2.7 %collective-permute-done.5.refs_2_ = bf16[1,1024,128]{2,1,0:T(8,128)(2,1)S(1)} collective-permute-done((bf16[1,1024,128]{2,1,0:T(8,128)(2,1)S(1)}, bf16[1,1024,128]{2,1,0:T(8,128)(2,1)S(1)}, u32[]{:S(2)}, u32[]{:S(2)}) %collective-permute-start.5) | collective-permute-done | bytes 262176 | tf_op jit(solution)/shard_map/ppermute | solution.py:223
  102.3 0.4 shard_map.90
  102.7 7.7 %all_to_all.37.parts_ref = bf16[8,64,128]{2,1,0:T(8,128)(2,1)S(1)} all-to-all(bf16[8,64,128]{2,1,0:T(8,128)(2,1)S(1)} %shard_map.90), channel_id=1, replica_groups={{34,35,32,33,2,3,0,1},{38,39,36,37,6,7,4,5},{42,43,40,41,10,11,8,9},{46..., dimensions={0} | all-to-all | bytes 262144 | tf_op jit(solution)/shard_map/all_to_all | solution.py:367
  110.4 0.2 shard_map.91
  110.6 14.8 %all_to_all.38 = bf16[16,8,128]{2,1,0:T(8,128)(2,1)S(1)} all-to-all(bf16[16,8,128]{2,1,0:T(8,128)(2,1)S(1)} %bitcast.16), channel_id=1, replica_groups={{512,576,640,704,768,832,896,960,0,64,128,192,256,320,384,448},{513,577..., dimensions={0} | all-to-all | bytes 65536 | tf_op jit(solution)/shard_map/all_to_all | solution.py:367
  125.4 0.3 shard_map.92
  125.7 12.1 %all_to_all.39.refs_0_ = f32[32,1,128]{2,1,0:T(1,128)S(1)} all-to-all(f32[32,1,128]{2,1,0:T(1,128)S(1)} %get-tuple-element.34), channel_id=1, replica_groups={{18,19,16,17,22,23,20,21,26,27,24,25,30,31,28,29,2,3,0,1,6,7,4,5,10,11,..., dimensions={0} | all-to-all | bytes 32768 | tf_op jit(solution)/shard_map/all_to_all | solution.py:367
  137.9 0.8 shard_map.93
Async XLA Ops:
  3.1 48.8 %collective-permute-start = (bf16[2,128,1024]{2,1,0:T(8,128)(2,1)}, bf16[2,128,1024]{2,1,0:T(8,128)(2,1)S(1)}, u32[]{:S(2)}, u32[]{:S(2)}) collective-permute-start(bf16[2,128,1024]{2,1,0:T(8,128)(2,1)} %get-tuple-element.25), channel_id=1, source_target_pairs={{0,1},{1,2},{2,3},{3,0},{4,5},{5,6},{6,7},{7,4},{8,9},{9,10},{10,1... | collective-permute-start | bytes 1572872 | tf_op jit(solution)/shard_map/ppermute | solution.py:223
  6.6 45.4 %collective-permute-start.1 = (bf16[2,128,1024]{2,1,0:T(8,128)(2,1)}, bf16[2,128,1024]{2,1,0:T(8,128)(2,1)S(1)}, u32[]{:S(2)}, u32[]{:S(2)}) collective-permute-start(bf16[2,128,1024]{2,1,0:T(8,128)(2,1)} %get-tuple-element.26), channel_id=1, source_target_pairs={{0,2},{1,3},{2,0},{3,1},{4,6},{5,7},{6,4},{7,5},{8,10},{9,11},{10,... | collective-permute-start | bytes 1572872 | tf_op jit(solution)/shard_map/ppermute | solution.py:223
  22.2 29.8 %collective-permute-start.2 = (bf16[2,128,1024]{2,1,0:T(8,128)(2,1)S(1)}, bf16[2,128,1024]{2,1,0:T(8,128)(2,1)S(1)}, u32[]{:S(2)}, u32[]{:S(2)}) collective-permute-start(bf16[2,128,1024]{2,1,0:T(8,128)(2,1)S(1)} %get-tuple-element.27), channel_id=1, source_target_pairs={{0,3},{1,0},{2,1},{3,2},{4,7},{5,4},{6,5},{7,6},{8,11},{9,8},{10,9... | collective-permute-start | bytes 1572872 | tf_op jit(solution)/shard_map/ppermute | solution.py:223
  24.1 19.2 %all-to-all-start = ((bf16[16,8,128]{2,1,0:T(8,128)(2,1)}), bf16[16,8,128]{2,1,0:T(8,128)(2,1)S(1)}, u32[]{:S(2)}, u32[]{:S(2)}) async-start(bf16[16,8,128]{2,1,0:T(8,128)(2,1)} %bitcast.2), calls=%async_computation | async-start | bytes 65536 | tf_op jit(solution)/shard_map/all_to_all | solution.py:367
  74.3 21.4 %all-to-all-start.3 = ((bf16[8,128,128]{2,1,0:T(8,128)(2,1)}), bf16[8,128,128]{2,1,0:T(8,128)(2,1)S(1)}, u32[]{:S(2)}, u32[]{:S(2)}) async-start(bf16[8,128,128]{2,1,0:T(8,128)(2,1)} %shard_map.86), calls=%async_computation.3 | async-start | bytes 524288 | tf_op jit(solution)/shard_map/all_to_all | solution.py:367
  83.0 11.8 %copy-start = (s32[2048,4]{0,1:T(4,128)S(1)}, s32[2048,4]{0,1:T(4,128)}, u32[]{:S(2)}) copy-start(s32[2048,4]{0,1:T(4,128)} %param.11) | copy-start | bytes 98308
  83.0 11.8 %copy-start.1 = (f32[2048,4]{0,1:T(4,128)S(1)}, f32[2048,4]{0,1:T(4,128)}, u32[]{:S(2)}) copy-start(f32[2048,4]{0,1:T(4,128)} %param.12) | copy-start | bytes 98308
  84.3 11.7 %collective-permute-start.3 = (bf16[1,1024,128]{2,1,0:T(8,128)(2,1)S(1)}, bf16[1,1024,128]{2,1,0:T(8,128)(2,1)S(1)}, u32[]{:S(2)}, u32[]{:S(2)}) collective-permute-start(bf16[1,1024,128]{2,1,0:T(8,128)(2,1)S(1)} %get-tuple-element.30), channel_id=1, source_target_pairs={{0,1},{1,2},{2,3},{3,0},{4,5},{5,6},{6,7},{7,4},{8,9},{9,10},{10,1... | collective-permute-start | bytes 786440 | tf_op jit(solution)/shard_map/ppermute | solution.py:223
  87.5 12.1 %collective-permute-start.4 = (bf16[1,1024,128]{2,1,0:T(8,128)(2,1)S(1)}, bf16[1,1024,128]{2,1,0:T(8,128)(2,1)S(1)}, u32[]{:S(2)}, u32[]{:S(2)}) collective-permute-start(bf16[1,1024,128]{2,1,0:T(8,128)(2,1)S(1)} %get-tuple-element.31), channel_id=1, source_target_pairs={{0,2},{1,3},{2,0},{3,1},{4,6},{5,7},{6,4},{7,5},{8,10},{9,11},{10,... | collective-permute-start | bytes 786440 | tf_op jit(solution)/shard_map/ppermute | solution.py:223
  90.6 11.8 %collective-permute-start.5 = (bf16[1,1024,128]{2,1,0:T(8,128)(2,1)S(1)}, bf16[1,1024,128]{2,1,0:T(8,128)(2,1)S(1)}, u32[]{:S(2)}, u32[]{:S(2)}) collective-permute-start(bf16[1,1024,128]{2,1,0:T(8,128)(2,1)S(1)} %get-tuple-element.32), channel_id=1, source_target_pairs={{0,3},{1,0},{2,1},{3,2},{4,7},{5,4},{6,5},{7,6},{8,11},{9,8},{10,9... | collective-permute-start | bytes 786440 | tf_op jit(solution)/shard_map/ppermute | solution.py:223
  94.8 0.7 copy-start.2

commit v5 on v4

--- a/solution.py
+++ b/solution.py
@@ -12,7 +12,7 @@
 CAP = 4
 GROUP = 8
 PARAMS = pltpu.CompilerParams(vmem_limit_bytes=16 * 1024 * 1024)
-FIRST = {"z": lambda n: 15, "c": lambda n: n - 1, "y": lambda n: n // 2, "x": lambda n: n // 2}
+FIRST = {"z": lambda n: 14, "c": lambda n: n - 1, "y": lambda n: n // 2, "x": lambda n: n // 2}
 STEP = {"z": 1, "c": 1, "y": 1, "x": 1}
 BACK = 8
 REDUCE = [4, 7, 2, 5, 0, 3, 6, 1]
@@ -216,6 +216,10 @@
 def select_step(routes_ref, gain_ref, sel_ref, tail_ref):
     select_table([routes_ref[:, k, :] for k in range(CAP)], sel_ref)
     tail_kernel(gain_ref, tail_ref)
+
+
+def tail_copy(in_ref, out_ref):
+    out_ref[...] = in_ref[...]
 
 
 def passed(piece, d, axis):
@@ -376,16 +380,17 @@
     weights = jnp.transpose(route_weights.reshape(chips, LANES, CAP), (0, 2, 1))
 
     square = shape((LANES, LANES), BF)
-    near, far, back, outgoing, place = deal(
-        [w_gate, w_up], [1, 2, 3], (dispatch_step,), (routes, tokens), (square, square), out=(1,)
-    )
-    own, sel, tail = deal(
+    near, far, outgoing, place = deal(
+        [w_gate, w_up], [1, 2], (dispatch_step,), (routes, tokens), (square, square), out=(1,)
+    )
+    own, back, sel, gains = deal(
         [w_gate, w_up],
-        [0],
+        [0, 3],
         (select_step,),
         (routes, in_gain.reshape(1, local)),
         (shape((CAP, LANES, LANES), BF), shape((8, LANES), BF)),
     )
+    tail = call(tail_copy, shape((8, LANES), BF), gains)
     gate_up = [own, passed(near, 1, "x"), passed(far, 2, "x"), passed(back, 3, "x")]
     own, near, far, back = deal([w_down], [0, 1, 2, 3])
     down = [own, passed(near, 1, "x"), passed(far, 2, "x"), passed(back, 3, "x")]

time: 139 us -> 140 us (level)
    pallas_call x9 -> x10, Pallas kernels: 3.9 us -> 3.9 us  [call(): pl.pallas_call(kernel, out_shape=outs, in_specs=[VMEM] * len(args), out_s...]
  transfers between devices with their start and end apart: 8 -> 8, of which waited for: 3 -> 3; matrix products, arithmetic and copies ran while one was open for 0% -> 0% of each run, Pallas kernels for 2% -> 3%
where the time goes in v5:
time: 140 us; the launch traced here: 139 us
  blocking collectives  63.3 us (45%)
  starting transfers between devices  49.9 us (36%)
  waiting for transfers between devices  15.6 us (11%)
  Pallas kernels  9.55 us (7%)
    all_to_all x5, blocking collectives, exchange(): lax.all_to_all(value, axes, 0, 0, tiled=True, axis_index_groups=groups)  63.3 us
    ppermute x6, starting transfers between devices, passed(): return lax.ppermute(piece, axis, [(i, (i + d) % n) for i in range(n)])  31.5 us
    all_to_all x2, starting transfers between devices, exchange(): lax.all_to_all(value, axes, 0, 0, tiled=True, axis_index_groups=groups)  18.4 us
    all_to_all x2, waiting for transfers between devices, exchange(): lax.all_to_all(value, axes, 0, 0, tiled=True, axis_index_groups=groups)  9.23 us
    ppermute x6, waiting for transfers between devices, passed(): return lax.ppermute(piece, axis, [(i, (i + d) % n) for i in range(n)])  6.35 us
    pallas_call x3, Pallas kernels, deal(): pl.pallas_call(body, out_shape=shapes, in_specs=[HBM] * (n + k), out_spec...  5.65 us
    pallas_call x10, Pallas kernels, call(): pl.pallas_call(kernel, out_shape=outs, in_specs=[VMEM] * len(args), out_s...  3.9 us
  transfers between devices with their start and end apart: 8, of which 3 were waited for; matrix products, arithmetic and copies ran while one was open for 0% of the time, Pallas kernels for 3%

profile of v5, /device:TPU:2, one launch (start us, length us, event | category | flops | bytes accessed | tf_op | source)
XLA Modules:
  0.0 139.1 jit_solution(18369285088682123964)
XLA Ops:
  0.0 1.5 %shard_map.83 = (bf16[2,128,1024]{2,1,0:T(8,128)(2,1)S(1)}, bf16[2,128,1024]{2,1,0:T(8,128)(2,1)S(1)}, bf16[4,128,128]{2,1,0:T(8,128)(2,1)S(1)}, bf16[8,128]{1,0:T(8,128)(2,1)S(1)}) custom-call(bf16[4,128,1024]{2,1,0:T(8,128)(2,1)} %refs_0_.4, bf16[4,128,1024]{2,1,0:T(8,128)(2,1)} %refs_1_.3, s32[16,4,128]{2,1,0:T(4,128)} %bitcast.12, f32[1,128]{1,0:T(1,128)} %bitcast.20), custom_call_target="tpu_custom_call" | custom-call | tf_op jit(solution)/shard_map/pallas_call | solution.py:130
  1.5 15.1 %collective-permute-start.2 = (bf16[2,128,1024]{2,1,0:T(8,128)(2,1)S(1)}, bf16[2,128,1024]{2,1,0:T(8,128)(2,1)S(1)}, u32[]{:S(2)}, u32[]{:S(2)}) collective-permute-start(bf16[2,128,1024]{2,1,0:T(8,128)(2,1)S(1)} %get-tuple-element.27), channel_id=1, source_target_pairs={{0,3},{1,0},{2,1},{3,2},{4,7},{5,4},{6,5},{7,6},{8,11},{9,8},{10,9... | collective-permute-start | bytes 1572872 | tf_op jit(solution)/shard_map/ppermute | solution.py:227
  16.6 2.9 %shard_map.82 = (bf16[2,128,1024]{2,1,0:T(8,128)(2,1)}, bf16[2,128,1024]{2,1,0:T(8,128)(2,1)}, bf16[128,128]{1,0:T(8,128)(2,1)}, bf16[128,128]{1,0:T(8,128)(2,1)S(1)}) custom-call(bf16[4,128,1024]{2,1,0:T(8,128)(2,1)} %refs_0_.4, bf16[4,128,1024]{2,1,0:T(8,128)(2,1)} %refs_1_.3, s32[16,4,128]{2,1,0:T(4,128)} %bitcast.13, bf16[64,128]{1,0:T(8,128)(2,1)} %refs_3_.1), custom_call_target="tpu_custom_call" | custom-call | tf_op jit(solution)/shard_map/pallas_call | solution.py:130
  19.5 1.9 %collective-permute-start = (bf16[2,128,1024]{2,1,0:T(8,128)(2,1)}, bf16[2,128,1024]{2,1,0:T(8,128)(2,1)S(1)}, u32[]{:S(2)}, u32[]{:S(2)}) collective-permute-start(bf16[2,128,1024]{2,1,0:T(8,128)(2,1)} %get-tuple-element.25), channel_id=1, source_target_pairs={{0,1},{1,2},{2,3},{3,0},{4,5},{5,6},{6,7},{7,4},{8,9},{9,10},{10,1... | collective-permute-start | bytes 1572872 | tf_op jit(solution)/shard_map/ppermute | solution.py:227
  21.4 4.0 %collective-permute-start.1 = (bf16[2,128,1024]{2,1,0:T(8,128)(2,1)}, bf16[2,128,1024]{2,1,0:T(8,128)(2,1)S(1)}, u32[]{:S(2)}, u32[]{:S(2)}) collective-permute-start(bf16[2,128,1024]{2,1,0:T(8,128)(2,1)} %get-tuple-element.26), channel_id=1, source_target_pairs={{0,2},{1,3},{2,0},{3,1},{4,6},{5,7},{6,4},{7,5},{8,10},{9,11},{10,... | collective-permute-start | bytes 1572872 | tf_op jit(solution)/shard_map/ppermute | solution.py:227
  25.4 9.7 %all-to-all-start = ((bf16[16,8,128]{2,1,0:T(8,128)(2,1)}), bf16[16,8,128]{2,1,0:T(8,128)(2,1)S(1)}, u32[]{:S(2)}, u32[]{:S(2)}) async-start(bf16[16,8,128]{2,1,0:T(8,128)(2,1)} %bitcast.2), calls=%async_computation | async-start | bytes 65536 | tf_op jit(solution)/shard_map/all_to_all | solution.py:371
  35.2 9.2 %all-to-all-done = bf16[16,8,128]{2,1,0:T(8,128)(2,1)S(1)} async-done(((bf16[16,8,128]{2,1,0:T(8,128)(2,1)}), bf16[16,8,128]{2,1,0:T(8,128)(2,1)S(1)}, u32[]{:S(2)}, u32[]{:S(2)}) %all-to-all-start) | async-done | bytes 32800 | tf_op jit(solution)/shard_map/all_to_all | solution.py:371
  44.4 0.2 shard_map.85
  44.6 7.6 %all_to_all.35.rows_ref = bf16[8,72,128]{2,1,0:T(8,128)(2,1)S(1)} all-to-all(bf16[8,72,128]{2,1,0:T(8,128)(2,1)S(1)} %shard_map.85), channel_id=1, replica_groups={{34,35,32,33,2,3,0,1},{38,39,36,37,6,7,4,5},{42,43,40,41,10,11,8,9},{46..., dimensions={0} | all-to-all | bytes 294912 | tf_op jit(solution)/shard_map/all_to_all | solution.py:371
  52.2 0.0 collective-permute-done.2.refs_3_
  52.2 0.0 collective-permute-done.refs_1_
  52.2 0.0 collective-permute-done.1.refs_2_
  52.2 0.7 shard_map.86
  52.9 20.8 %all_to_all.36.refs_0_ = bf16[8,264,128]{2,1,0:T(8,128)(2,1)S(1)} all-to-all(bf16[8,264,128]{2,1,0:T(8,128)(2,1)S(1)} %shard_map.86), channel_id=1, replica_groups={{16,28,8,20,0,12,24,4},{17,29,9,21,1,13,25,5},{18,30,10,22,2,14,26,6},{..., dimensions={0} | all-to-all | bytes 1081344 | tf_op jit(solution)/shard_map/all_to_all | solution.py:371
  73.7 0.9 shard_map.87
  74.6 8.7 %all-to-all-start.3 = ((bf16[8,128,128]{2,1,0:T(8,128)(2,1)}), bf16[8,128,128]{2,1,0:T(8,128)(2,1)S(1)}, u32[]{:S(2)}, u32[]{:S(2)}) async-start(bf16[8,128,128]{2,1,0:T(8,128)(2,1)} %shard_map.87), calls=%async_computation.3 | async-start | bytes 524288 | tf_op jit(solution)/shard_map/all_to_all | solution.py:371
  83.3 0.0 copy-start
  83.3 0.0 copy-start.1
  83.3 1.2 shard_map.89
  84.5 3.3 %collective-permute-start.3 = (bf16[1,1024,128]{2,1,0:T(8,128)(2,1)S(1)}, bf16[1,1024,128]{2,1,0:T(8,128)(2,1)S(1)}, u32[]{:S(2)}, u32[]{:S(2)}) collective-permute-start(bf16[1,1024,128]{2,1,0:T(8,128)(2,1)S(1)} %get-tuple-element.30), channel_id=1, source_target_pairs={{0,1},{1,2},{2,3},{3,0},{4,5},{5,6},{6,7},{7,4},{8,9},{9,10},{10,1... | collective-permute-start | bytes 786440 | tf_op jit(solution)/shard_map/ppermute | solution.py:227
  87.8 3.0 %collective-permute-start.4 = (bf16[1,1024,128]{2,1,0:T(8,128)(2,1)S(1)}, bf16[1,1024,128]{2,1,0:T(8,128)(2,1)S(1)}, u32[]{:S(2)}, u32[]{:S(2)}) collective-permute-start(bf16[1,1024,128]{2,1,0:T(8,128)(2,1)S(1)} %get-tuple-element.31), channel_id=1, source_target_pairs={{0,2},{1,3},{2,0},{3,1},{4,6},{5,7},{6,4},{7,5},{8,10},{9,11},{10,... | collective-permute-start | bytes 786440 | tf_op jit(solution)/shard_map/ppermute | solution.py:227
  90.8 4.3 %collective-permute-start.5 = (bf16[1,1024,128]{2,1,0:T(8,128)(2,1)S(1)}, bf16[1,1024,128]{2,1,0:T(8,128)(2,1)S(1)}, u32[]{:S(2)}, u32[]{:S(2)}) collective-permute-start(bf16[1,1024,128]{2,1,0:T(8,128)(2,1)S(1)} %get-tuple-element.32), channel_id=1, source_target_pairs={{0,3},{1,0},{2,1},{3,2},{4,7},{5,4},{6,5},{7,6},{8,11},{9,8},{10,9... | collective-permute-start | bytes 786440 | tf_op jit(solution)/shard_map/ppermute | solution.py:227
  95.1 0.0 copy-start.2
  95.1 0.0 copy-done
  95.1 0.0 copy-done.1
  95.1 0.6 copy-done.2
  95.7 0.2 shard_map.88
  96.0 0.0 all-to-all-done.3.act_ref
  96.0 0.2 shard_map.90.own_ref
  96.2 0.0 collective-permute-done.3.refs_0_
  96.2 3.6 %collective-permute-done.4.refs_1_ = bf16[1,1024,128]{2,1,0:T(8,128)(2,1)S(1)} collective-permute-done((bf16[1,1024,128]{2,1,0:T(8,128)(2,1)S(1)}, bf16[1,1024,128]{2,1,0:T(8,128)(2,1)S(1)}, u32[]{:S(2)}, u32[]{:S(2)}) %collective-permute-start.4) | collective-permute-done | bytes 262176 | tf_op jit(solution)/shard_map/ppermute | solution.py:227
  99.9 2.7 %collective-permute-done.5.refs_2_ = bf16[1,1024,128]{2,1,0:T(8,128)(2,1)S(1)} collective-permute-done((bf16[1,1024,128]{2,1,0:T(8,128)(2,1)S(1)}, bf16[1,1024,128]{2,1,0:T(8,128)(2,1)S(1)}, u32[]{:S(2)}, u32[]{:S(2)}) %collective-permute-start.5) | collective-permute-done | bytes 262176 | tf_op jit(solution)/shard_map/ppermute | solution.py:227
  102.6 0.4 shard_map.91
  102.9 7.7 %all_to_all.37.parts_ref = bf16[8,64,128]{2,1,0:T(8,128)(2,1)S(1)} all-to-all(bf16[8,64,128]{2,1,0:T(8,128)(2,1)S(1)} %shard_map.91), channel_id=1, replica_groups={{34,35,32,33,2,3,0,1},{38,39,36,37,6,7,4,5},{42,43,40,41,10,11,8,9},{46..., dimensions={0} | all-to-all | bytes 262144 | tf_op jit(solution)/shard_map/all_to_all | solution.py:371
  110.7 0.2 shard_map.92
  110.9 15.1 %all_to_all.38 = bf16[16,8,128]{2,1,0:T(8,128)(2,1)S(1)} all-to-all(bf16[16,8,128]{2,1,0:T(8,128)(2,1)S(1)} %bitcast.16), channel_id=1, replica_groups={{512,576,640,704,768,832,896,960,0,64,128,192,256,320,384,448},{513,577..., dimensions={0} | all-to-all | bytes 65536 | tf_op jit(solution)/shard_map/all_to_all | solution.py:371
  125.9 0.3 shard_map.93
  126.2 12.1 %all_to_all.39.refs_0_ = f32[32,1,128]{2,1,0:T(1,128)S(1)} all-to-all(f32[32,1,128]{2,1,0:T(1,128)S(1)} %get-tuple-element.34), channel_id=1, replica_groups={{18,19,16,17,22,23,20,21,26,27,24,25,30,31,28,29,2,3,0,1,6,7,4,5,10,11,..., dimensions={0} | all-to-all | bytes 32768 | tf_op jit(solution)/shard_map/all_to_all | solution.py:371
  138.4 0.8 shard_map.94
  (1 shorter events, 0.0 us)
Async XLA Ops:
  1.5 50.7 %collective-permute-start.2 = (bf16[2,128,1024]{2,1,0:T(8,128)(2,1)S(1)}, bf16[2,128,1024]{2,1,0:T(8,128)(2,1)S(1)}, u32[]{:S(2)}, u32[]{:S(2)}) collective-permute-start(bf16[2,128,1024]{2,1,0:T(8,128)(2,1)S(1)} %get-tuple-element.27), channel_id=1, source_target_pairs={{0,3},{1,0},{2,1},{3,2},{4,7},{5,4},{6,5},{7,6},{8,11},{9,8},{10,9... | collective-permute-start | bytes 1572872 | tf_op jit(solution)/shard_map/ppermute | solution.py:227
  19.5 32.7 %collective-permute-start = (bf16[2,128,1024]{2,1,0:T(8,128)(2,1)}, bf16[2,128,1024]{2,1,0:T(8,128)(2,1)S(1)}, u32[]{:S(2)}, u32[]{:S(2)}) collective-permute-start(bf16[2,128,1024]{2,1,0:T(8,128)(2,1)} %get-tuple-element.25), channel_id=1, source_target_pairs={{0,1},{1,2},{2,3},{3,0},{4,5},{5,6},{6,7},{7,4},{8,9},{9,10},{10,1... | collective-permute-start | bytes 1572872 | tf_op jit(solution)/shard_map/ppermute | solution.py:227
  21.4 30.8 %collective-permute-start.1 = (bf16[2,128,1024]{2,1,0:T(8,128)(2,1)}, bf16[2,128,1024]{2,1,0:T(8,128)(2,1)S(1)}, u32[]{:S(2)}, u32[]{:S(2)}) collective-permute-start(bf16[2,128,1024]{2,1,0:T(8,128)(2,1)} %get-tuple-element.26), channel_id=1, source_target_pairs={{0,2},{1,3},{2,0},{3,1},{4,6},{5,7},{6,4},{7,5},{8,10},{9,11},{10,... | collective-permute-start | bytes 1572872 | tf_op jit(solution)/shard_map/ppermute | solution.py:227
  25.4 19.0 %all-to-all-start = ((bf16[16,8,128]{2,1,0:T(8,128)(2,1)}), bf16[16,8,128]{2,1,0:T(8,128)(2,1)S(1)}, u32[]{:S(2)}, u32[]{:S(2)}) async-start(bf16[16,8,128]{2,1,0:T(8,128)(2,1)} %bitcast.2), calls=%async_computation | async-start | bytes 65536 | tf_op jit(solution)/shard_map/all_to_all | solution.py:371
  74.6 21.4 %all-to-all-start.3 = ((bf16[8,128,128]{2,1,0:T(8,128)(2,1)}), bf16[8,128,128]{2,1,0:T(8,128)(2,1)S(1)}, u32[]{:S(2)}, u32[]{:S(2)}) async-start(bf16[8,128,128]{2,1,0:T(8,128)(2,1)} %shard_map.87), calls=%async_computation.3 | async-start | bytes 524288 | tf_op jit(solution)/shard_map/all_to_all | solution.py:371
  83.3 11.8 %copy-start = (s32[2048,4]{0,1:T(4,128)S(1)}, s32[2048,4]{0,1:T(4,128)}, u32[]{:S(2)}) copy-start(s32[2048,4]{0,1:T(4,128)} %param.11) | copy-start | bytes 98308
  83.3 11.8 %copy-start.1 = (f32[2048,4]{0,1:T(4,128)S(1)}, f32[2048,4]{0,1:T(4,128)}, u32[]{:S(2)}) copy-start(f32[2048,4]{0,1:T(4,128)} %param.12) | copy-start | bytes 98308
  84.5 11.7 %collective-permute-start.3 = (bf16[1,1024,128]{2,1,0:T(8,128)(2,1)S(1)}, bf16[1,1024,128]{2,1,0:T(8,128)(2,1)S(1)}, u32[]{:S(2)}, u32[]{:S(2)}) collective-permute-start(bf16[1,1024,128]{2,1,0:T(8,128)(2,1)S(1)} %get-tuple-element.30), channel_id=1, source_target_pairs={{0,1},{1,2},{2,3},{3,0},{4,5},{5,6},{6,7},{7,4},{8,9},{9,10},{10,1... | collective-permute-start | bytes 786440 | tf_op jit(solution)/shard_map/ppermute | solution.py:227
  87.8 12.1 %collective-permute-start.4 = (bf16[1,1024,128]{2,1,0:T(8,128)(2,1)S(1)}, bf16[1,1024,128]{2,1,0:T(8,128)(2,1)S(1)}, u32[]{:S(2)}, u32[]{:S(2)}) collective-permute-start(bf16[1,1024,128]{2,1,0:T(8,128)(2,1)S(1)} %get-tuple-element.31), channel_id=1, source_target_pairs={{0,2},{1,3},{2,0},{3,1},{4,6},{5,7},{6,4},{7,5},{8,10},{9,11},{10,... | collective-permute-start | bytes 786440 | tf_op jit(solution)/shard_map/ppermute | solution.py:227
  90.8 11.8 %collective-permute-start.5 = (bf16[1,1024,128]{2,1,0:T(8,128)(2,1)S(1)}, bf16[1,1024,128]{2,1,0:T(8,128)(2,1)S(1)}, u32[]{:S(2)}, u32[]{:S(2)}) collective-permute-start(bf16[1,1024,128]{2,1,0:T(8,128)(2,1)S(1)} %get-tuple-element.32), channel_id=1, source_target_pairs={{0,3},{1,0},{2,1},{3,2},{4,7},{5,4},{6,5},{7,6},{8,11},{9,8},{10,9... | collective-permute-start | bytes 786440 | tf_op jit(solution)/shard_map/ppermute | solution.py:227
  95.1 0.7 copy-start.2
